TPU v7x, 32 devices: a whole 2x2x4 slice. The times are simulated.
32 devices in a mesh: grp: 2 (over x), st: 4 (over y, core), tp: 4 (over z).
Axes of the slice: x: 2, y: 2, z: 4, core: 2. Of those that a mesh axis runs over, the one named last changes fastest.
Arguments:
- tokens: bfloat16 [2048, 2048], P(('grp', 'st')), parts along dimension 0, may hold values from -6 to 6
- pre_gain: float32 [2048], replicated, may hold values from 0.1 to 1.9
- w_gated: bfloat16 [2048, 1536], P(None, 'tp'), may hold values from -0.125 to 0.125
- w_mixed: bfloat16 [2048, 1536], P(None, 'tp'), may hold values from -0.125 to 0.125
- mix_weight: bfloat16 [8, 128, 128], P('tp'), may hold values from -0.5 to 0.5
- w_query: bfloat16 [2048, 1024], P(None, 'tp'), may hold values from -0.125 to 0.125
- w_gate_mix: bfloat16 [2048, 1536], P(None, 'tp'), may hold values from -0.125 to 0.125
- w_gate_read: bfloat16 [2048, 1024], P(None, 'tp'), may hold values from -0.125 to 0.125
- store: bfloat16 [64, 128, 2048], P(('grp', 'st')), parts along dimension 0, may hold values from -6 to 6
- mem_gain: float32 [2048], replicated, may hold values from 1 to 80
- w_key: bfloat16 [2048, 1024], P(None, 'tp'), may hold values from -0.125 to 0.125
- w_value: bfloat16 [2048, 1024], P(None, 'tp'), may hold values from -0.125 to 0.125
- passage_ids: int32 [32, 4], P(('grp', 'st')), parts along dimension 0, may hold values from 0 to 31, as said below
- w_out_mix: bfloat16 [1536, 2048], P('tp'), may hold values from -0.125 to 0.125
- w_out_read: bfloat16 [1024, 2048], P('tp'), may hold values from -0.125 to 0.125
Outputs:
- mixed_out: bfloat16 [2048, 2048], P(('grp', 'st', 'tp')), parts along dimension 0
There are 2 independent parts, one for each index of `grp`. A program takes and returns all parts, laid end to end along the dimension named above; an argument that names none is the same for every part. Nothing has to cross between parts.
Inputs may be any that keep to these rules, and one draw needn't show every extreme that they name: `passage_ids`: passage p is held by index p // 8 of st. The 16 entries of one index of st name at most 8 passages held by any one index of st, and that most is reached in every draw.
All inputs are finite; a program needn't handle non-finite values.
Results may differ from a plain program's by a relative error of at most 0.015.
The roundings to bfloat16 on the way count: a program that leaves them out, or rounds other values in their place, can miss the bound.
Values may be sent and summed in bfloat16 or wider, within the bound.
No kernel may reach another device: no remote copies, remote signals or barrier semaphores. Data moves between devices by JAX's collectives and lax.ppermute only.
A program may use at most 128 MiB of HBM per device.

v0:
```python
import jax
import jax.numpy as jnp
from jax import lax
from jax.sharding import PartitionSpec as P

HD = 128
SPAN = 128
RBLOCK = 64
NPB = 4
PROWS = 128


eps = 1e-06


def row_norm(values_in, gain):
    widened = values_in.astype(jnp.float32)
    return (
        widened * lax.rsqrt(jnp.mean(widened * widened, axis=-1, keepdims=True) + eps) * gain
    ).astype(jnp.bfloat16)


def local(
    tokens,
    pre_gain,
    w_gated,
    w_mixed,
    mix_weight,
    w_query,
    w_gate_mix,
    w_gate_read,
    store,
    mem_gain,
    w_key,
    w_value,
    passage_ids,
    w_out_mix,
    w_out_read,
):
    tok_rows = tokens.shape[0]
    st_count = lax.axis_size("st")
    normed = row_norm(tokens, pre_gain)
    gated = jnp.dot(normed, w_gated, preferred_element_type=jnp.float32)
    mixed_in = jnp.dot(normed, w_mixed, preferred_element_type=jnp.float32)
    groups_here = mix_weight.shape[0]
    group_width = mixed_in.shape[1] // groups_here
    grouped = mixed_in.reshape(tok_rows, groups_here, group_width)
    group_mean = jnp.mean(grouped, axis=-1, keepdims=True)
    centred = grouped - group_mean
    group_var = jnp.mean(centred * centred, axis=-1, keepdims=True)
    mixed_norm = (centred * lax.rsqrt(group_var + eps)).astype(jnp.bfloat16)
    causal = jnp.tril(jnp.ones((SPAN, SPAN), dtype=bool))
    mix_masked = jnp.where(causal[None], mix_weight, jnp.zeros_like(mix_weight))
    blocked = mixed_norm.reshape(tok_rows // SPAN, SPAN, groups_here, group_width)
    spatial = jnp.einsum(
        "hts,nshd->nthd", mix_masked, blocked, preferred_element_type=jnp.float32
    ).reshape(tok_rows, -1)
    branch_mix = gated * spatial
    query = jnp.dot(normed, w_query, preferred_element_type=jnp.float32).astype(jnp.bfloat16)
    head_width = w_query.shape[1]
    heads_here = head_width // HD
    flat_ids = passage_ids.reshape(-1)
    req_count = flat_ids.shape[0]
    per_owner = store.shape[0]
    capacity = max(2, (2 * req_count + st_count - 1) // st_count)
    owner = flat_ids // per_owner
    local_id = flat_ids - owner * per_owner
    position = jnp.arange(req_count, dtype=jnp.int32)
    same_owner = owner[:, None] == owner[None, :]
    earlier = position[None, :] < position[:, None]
    rank = jnp.sum((same_owner & earlier).astype(jnp.int32), axis=1)
    slot = owner * capacity + rank
    slot_range = jnp.arange(st_count * capacity, dtype=jnp.int32)
    table = jnp.sum(jnp.where(slot[:, None] == slot_range[None, :], local_id[:, None], 0), axis=0)
    table = table.reshape(st_count, capacity)
    held_rows = row_norm(store, mem_gain).reshape(-1, store.shape[-1])
    key_store = (
        jnp.dot(held_rows, w_key, preferred_element_type=jnp.float32)
        .astype(jnp.bfloat16)
        .reshape(per_owner, PROWS, head_width)
    )
    value_store = (
        jnp.dot(held_rows, w_value, preferred_element_type=jnp.float32)
        .astype(jnp.bfloat16)
        .reshape(per_owner, PROWS, head_width)
    )
    wanted = lax.all_to_all(table, "st", split_axis=0, concat_axis=0, tiled=True)
    arrived = (
        lax.all_to_all(key_store[wanted], "st", split_axis=0, concat_axis=0, tiled=True),
        lax.all_to_all(value_store[wanted], "st", split_axis=0, concat_axis=0, tiled=True),
    )
    blocks_here = tok_rows // RBLOCK
    key_slots, value_slots = arrived
    keys = key_slots.reshape(st_count * capacity, PROWS, head_width)[slot]
    values = value_slots.reshape(st_count * capacity, PROWS, head_width)[slot]
    keys = keys.reshape(blocks_here, NPB * PROWS, heads_here, HD)
    values = values.reshape(blocks_here, NPB * PROWS, heads_here, HD)
    query_blocks = query.reshape(blocks_here, RBLOCK, heads_here, HD)
    scores = jnp.einsum(
        "btha,bkha->bhtk", query_blocks, keys, preferred_element_type=jnp.float32
    ) * HD ** (-0.5)
    probs = jax.nn.softmax(scores, axis=-1).astype(jnp.bfloat16)
    branch_read = jnp.einsum(
        "bhtk,bkha->btha", probs, values, preferred_element_type=jnp.float32
    ).reshape(tok_rows, head_width)
    gate_mix = jnp.dot(normed, w_gate_mix, preferred_element_type=jnp.float32)
    gate_read = jnp.dot(normed, w_gate_read, preferred_element_type=jnp.float32)
    out_mix = (branch_mix * jax.nn.silu(gate_mix)).astype(jnp.bfloat16)
    out_read = (branch_read * jax.nn.silu(gate_read)).astype(jnp.bfloat16)
    return lax.psum_scatter(
        (
            jnp.dot(out_mix, w_out_mix, preferred_element_type=jnp.float32)
            + jnp.dot(out_read, w_out_read, preferred_element_type=jnp.float32)
        ).astype(jnp.bfloat16),
        "tp",
        scatter_dimension=0,
        tiled=True,
    )


def solution(mesh):
    placed = (
        P(("grp", "st"), None),
        P(),
        P(None, "tp"),
        P(None, "tp"),
        P("tp", None, None),
        P(None, "tp"),
        P(None, "tp"),
        P(None, "tp"),
        P(("grp", "st"), None, None),
        P(),
        P(None, "tp"),
        P(None, "tp"),
        P(("grp", "st"), None),
        P("tp", None),
        P("tp", None),
    )
    return jax.shard_map(
        local, mesh=mesh, in_specs=placed, out_specs=P(("grp", "st", "tp"), None), check_vma=False
    )
```

profile of v0, /device:TPU:0, one launch (start us, length us, event | category | flops | bytes accessed | tf_op | source)
XLA Modules:
  0.0 134.3 jit_solution(756137485507767994)
XLA Ops:
  6.5 0.9 reshape.281
  8.2 0.7 all_to_all.14
  8.9 4.3 %all-to-all-start = ((s32[4,1,8]{2,1,0:T(1,128)}), s32[4,1,8]{2,1,0:T(1,128)S(1)}, u32[]{:S(2)}, u32[]{:S(2)}) async-start(s32[4,1,8]{2,1,0:T(1,128)} %bitcast.6), calls=%async_computation | async-start | bytes 4096 | tf_op jit(solution)/shard_map/all_to_all | solution.py:87
  13.2 1.5 %fusion.5 = f32[256]{0:T(256)S(1)} fusion(bf16[256,2048]{1,0:T(8,128)(2,1)} %param.15), kind=kLoop, calls=%fused_computation.14 | loop fusion | flops 1572608 | bytes 1049600 | tf_op jit(solution)/shard_map/reduce_sum | solution.py:19
  14.7 3.2 %fusion.1 = f32[8,128]{1,0:T(8,128)S(1)} fusion(bf16[8,128,2048]{2,1,0:T(8,128)(2,1)} %param.23), kind=kLoop, calls=%fused_computation.7 | loop fusion | flops 6290432 | bytes 4198400 | tf_op jit(solution)/shard_map/reduce_sum | solution.py:19
  18.1 1.0 fusion.3
  19.3 1.2 convolution_convert_fusion
  21.2 2.0 %gather_fusion.2 = bf16[32,128,256]{2,1,0:T(8,128)(2,1)} fusion(bf16[8,128,256]{2,1,0:T(8,128)(2,1)S(1)} %bitcast.55, s32[1024]{0:T(1024)S(1)} %pad_clamp_fusion.1), kind=kCustom, calls=%fused_computation.2 | custom fusion | bytes 4194432 | tf_op jit(solution)/shard_map/gather | solution.py:89
  23.2 4.6 %all-to-all-start.2 = ((bf16[4,8,128,256]{3,2,1,0:T(8,128)(2,1)}), bf16[4,8,128,256]{3,2,1,0:T(8,128)(2,1)}, u32[]{:S(2)}, u32[]{:S(2)}) async-start(bf16[4,8,128,256]{3,2,1,0:T(8,128)(2,1)} %bitcast.54), calls=%async_computation.2 | async-start | bytes 4194304 | tf_op jit(solution)/shard_map/all_to_all | solution.py:89
  27.8 2.2 %fusion.42 = f32[256,384]{0,1:T(8,128)S(1)} fusion(bf16[2048,384]{1,0:T(8,128)(2,1)} %param.18, bf16[256,2048]{1,0:T(8,128)(2,1)S(1)} %copy-done.4, f32[2048]{0:T(1024)S(1)} %copy-done.11, f32[256]{0:T(256)S(1)} %add_rsqrt_fusion.2), kind=kOutput, calls=%fused_computation.82 | convolution fusion | flops 404750336 | bytes 3023872 | tf_op jit(solution)/shard_map/dot_general | solution.py:44
  31.4 2.4 %convolution_convert_fusion.2 = bf16[256,256]{1,0:T(8,128)(2,1)} fusion(bf16[2048,256]{1,0:T(8,128)(2,1)} %param.20, bf16[256,2048]{1,0:T(8,128)(2,1)S(1)} %copy-done.4, f32[2048]{0:T(1024)S(1)} %copy-done.11, f32[256]{0:T(256)S(1)} %add_rsqrt_fusion.2), kind=kOutput, calls=%fused_computation.27 | convolution fusion | flops 270598144 | bytes 2237440 | tf_op jit(solution)/shard_map/dot_general | solution.py:59
  33.7 3.4 %convolution_convert_fusion.1 = bf16[1024,256]{1,0:T(8,128)(2,1)S(1)} fusion(bf16[1024,2048]{1,0:T(8,128)(2,1)} %bitcast.58, bf16[2048,256]{1,0:T(8,128)(2,1)S(1)} %copy-done.17), kind=kOutput, calls=%fused_computation.21 | convolution fusion | flops 1074003968 | bytes 5767168 | tf_op jit(solution)/shard_map/dot_general | solution.py:83
  37.2 2.0 %gather_fusion = bf16[32,128,256]{2,1,0:T(8,128)(2,1)} fusion(bf16[8,128,256]{2,1,0:T(8,128)(2,1)S(1)} %bitcast.56, s32[1024]{0:T(1024)S(1)} %pad_clamp_fusion.1), kind=kCustom, calls=%fused_computation | custom fusion | bytes 4194432 | tf_op jit(solution)/shard_map/gather | solution.py:90
  39.2 14.3 %all-to-all-done.2 = bf16[4,8,128,256]{3,2,1,0:T(8,128)(2,1)} async-done(((bf16[4,8,128,256]{3,2,1,0:T(8,128)(2,1)}), bf16[4,8,128,256]{3,2,1,0:T(8,128)(2,1)}, u32[]{:S(2)}, u32[]{:S(2)}) %all-to-all-start.2) | async-done | bytes 2097184 | tf_op jit(solution)/shard_map/all_to_all | solution.py:89
  53.6 4.6 %all-to-all-start.1 = ((bf16[4,8,128,256]{3,2,1,0:T(8,128)(2,1)}), bf16[4,8,128,256]{3,2,1,0:T(8,128)(2,1)}, u32[]{:S(2)}, u32[]{:S(2)}) async-start(bf16[4,8,128,256]{3,2,1,0:T(8,128)(2,1)} %bitcast.53), calls=%async_computation.1 | async-start | bytes 4194304 | tf_op jit(solution)/shard_map/all_to_all | solution.py:90
  59.9 0.7 reshape.285
  60.5 0.7 rsqrt.29
  61.2 0.9 multiply_convert_fusion
  62.1 1.0 convolution_bitcast_fusion
  63.8 0.6 fusion.32
  64.4 3.0 %fusion.40 = f32[256,384]{1,0:T(8,128)} fusion(bf16[2048,384]{1,0:T(8,128)(2,1)} %param.21, bf16[256,2048]{1,0:T(8,128)(2,1)S(1)} %copy-done.4, f32[2048]{0:T(1024)} %param.16, f32[256]{0:T(256)} %copy-done.14), kind=kOutput, calls=%fused_computation.81 | convolution fusion | flops 404750336 | bytes 3023872 | tf_op jit(solution)/shard_map/dot_general | solution.py:106
  67.4 2.2 %gather_fusion.3 = bf16[16,128,256]{2,1,0:T(8,128)(2,1)S(1)} fusion(bf16[32,128,256]{2,1,0:T(8,128)(2,1)} %bitcast.14, s32[1024]{0:T(1024)S(1)} %pad_clamp_fusion), kind=kCustom, calls=%fused_computation.3 | custom fusion | bytes 2097216 | tf_op jit(solution)/shard_map/gather | solution.py:94
  69.6 1.1 reshape.288
  70.8 1.7 %convolution_multiply_fusion = f32[4,2,64,512]{3,2,1,0:T(8,128)S(1)} fusion(bf16[4,512,2,128]{3,2,1,0:T(2,128)(2,1)} %reshape.288, bf16[4,64,2,128]{3,2,1,0:T(2,128)(2,1)S(1)} %copy-done.6), kind=kOutput, calls=%fused_computation.19 | convolution fusion | flops 67371008 | bytes 2228224 | tf_op jit(solution)/shard_map/btha,bkha->bhtk/dot_general | solution.py:99
  72.5 1.0 copy-done.3
  73.8 10.1 %all-to-all-done.1 = bf16[4,8,128,256]{3,2,1,0:T(8,128)(2,1)} async-done(((bf16[4,8,128,256]{3,2,1,0:T(8,128)(2,1)}), bf16[4,8,128,256]{3,2,1,0:T(8,128)(2,1)}, u32[]{:S(2)}, u32[]{:S(2)}) %all-to-all-start.1) | async-done | bytes 2097184 | tf_op jit(solution)/shard_map/all_to_all | solution.py:90
  83.9 2.2 %gather_fusion.1 = bf16[16,128,256]{2,1,0:T(8,128)(2,1)S(1)} fusion(bf16[32,128,256]{2,1,0:T(8,128)(2,1)} %bitcast.9, s32[1024]{0:T(1024)S(1)} %pad_clamp_fusion), kind=kCustom, calls=%fused_computation.1 | custom fusion | bytes 2097216 | tf_op jit(solution)/shard_map/gather | solution.py:95
  86.1 1.1 reshape.284
  87.2 2.9 %convolution_bitcast_fusion.1 = f32[4,64,2,128]{3,1,2,0:T(8,128)S(1)} fusion(bf16[4,512,2,128]{3,2,1,0:T(2,128)(2,1)} %reshape.284, f32[4,2,64]{2,1,0:T(2,128)S(1)} %fusion.50, f32[4,2,64,512]{3,2,1,0:T(8,128)} %copy-done.3), kind=kOutput, calls=%fused_computation.26 | convolution fusion | flops 67896320 | bytes 2361344 | tf_op jit(solution)/shard_map/bhtk,bkha->btha/dot_general | solution.py:103
  90.4 4.2 %fusion.23 = f32[256,2048]{1,0:T(8,128)} fusion(bf16[256,2048]{1,0:T(8,128)(2,1)} %param.29, f32[32,8,2,128]{3,2,1,0:T(2,128)S(1)} %bitcast.61, bf16[2048,256]{1,0:T(8,128)(2,1)} %param.22, bf16[256,2048]{1,0:T(8,128)(2,1)S(1)} %copy-done.5, f32[2048]{0:T(1024)S(1)} %copy-done.12, f32[256]{0:T(256)S(1)} %copy-done.15), kind=kOutput, calls=%fused_computation.43 | convolution fusion | flops 539361280 | bytes 5514240 | tf_op jit(solution)/shard_map/dot_general | solution.py:113
  94.6 4.6 %fusion.4 = bf16[256,2048]{1,0:T(8,128)(2,1)} fusion(f32[256,2048]{1,0:T(8,128)} %fusion.23, bf16[384,2048]{1,0:T(8,128)(2,1)S(1)} %copy-done, f32[256,384]{1,0:T(8,128)S(1)} %reshape.325, bf16[2048,384]{1,0:T(8,128)(2,1)} %param.17, f32[256,384]{1,0:T(8,128)} %fusion.40, bf16[256,2048]{1,0:T(8,128)(2,1)S(1)} %copy-done.5, f32[2048]{0:T(1024)S(1)} %copy-done.12, ...), kind=kOutput, calls=%fused_computation.13 | convolution fusion | flops 809140224 | bytes 8135680 | tf_op jit(solution)/shard_map/dot_general | solution.py:112
  99.3 28.1 %reduce-scatter.2.cloned.1.call-done = bf16[64,2048]{1,0:T(8,128)(2,1)} async-done(((bf16[256,2048]{1,0:T(8,128)(2,1)}), bf16[64,2048]{1,0:T(8,128)(2,1)}) %reduce-scatter.2.cloned.1.call-update) | async-done | bytes 262160 | tf_op jit(solution)/shard_map/reduce_scatter | solution.py:110
  (62 shorter events, 5.9 us)
Async XLA Ops:
  6.5 88.1 %copy-start = (bf16[384,2048]{1,0:T(8,128)(2,1)S(1)}, bf16[384,2048]{1,0:T(8,128)(2,1)}, u32[]{:S(2)}) copy-start(bf16[384,2048]{1,0:T(8,128)(2,1)} %param.28) | copy-start | bytes 4718596
  7.6 0.5 copy-start.18
  8.9 12.2 %all-to-all-start = ((s32[4,1,8]{2,1,0:T(1,128)}), s32[4,1,8]{2,1,0:T(1,128)S(1)}, u32[]{:S(2)}, u32[]{:S(2)}) async-start(s32[4,1,8]{2,1,0:T(1,128)} %bitcast.6), calls=%async_computation | async-start | bytes 4096 | tf_op jit(solution)/shard_map/all_to_all | solution.py:87
  14.7 3.5 %copy-start.1 = (bf16[8,128,2048]{2,1,0:T(8,128)(2,1)S(1)}, bf16[8,128,2048]{2,1,0:T(8,128)(2,1)}, u32[]{:S(2)}) copy-start(bf16[8,128,2048]{2,1,0:T(8,128)(2,1)} %param.23) | copy-start | bytes 12582916
  14.7 3.4 %copy-start.10 = (f32[2048]{0:T(1024)S(1)}, f32[2048]{0:T(1024)}, u32[]{:S(2)}) copy-start(f32[2048]{0:T(1024)} %param.24) | copy-start | bytes 24580
  18.1 1.2 copy-start.16
  19.1 1.9 %copy-start.2 = (bf16[8,128,2048]{2,1,0:T(8,128)(2,1)}, bf16[8,128,2048]{2,1,0:T(8,128)(2,1)S(1)}, u32[]{:S(2)}) copy-start(bf16[8,128,2048]{2,1,0:T(8,128)(2,1)S(1)} %fusion.3) | copy-start | bytes 12582916
  21.1 10.3 %copy-start.14 = (f32[256]{0:T(256)}, f32[256]{0:T(256)S(1)}, u32[]{:S(2)}) copy-start(f32[256]{0:T(256)S(1)} %add_rsqrt_fusion.2) | copy-start | bytes 3076
  23.2 4.6 %copy-start.4 = (bf16[256,2048]{1,0:T(8,128)(2,1)S(1)}, bf16[256,2048]{1,0:T(8,128)(2,1)}, u32[]{:S(2)}) copy-start(bf16[256,2048]{1,0:T(8,128)(2,1)} %param.15) | copy-start | bytes 3145732
  23.2 4.6 %copy-start.11 = (f32[2048]{0:T(1024)S(1)}, f32[2048]{0:T(1024)}, u32[]{:S(2)}) copy-start(f32[2048]{0:T(1024)} %param.16) | copy-start | bytes 24580
  23.2 30.3 %all-to-all-start.2 = ((bf16[4,8,128,256]{3,2,1,0:T(8,128)(2,1)}), bf16[4,8,128,256]{3,2,1,0:T(8,128)(2,1)}, u32[]{:S(2)}, u32[]{:S(2)}) async-start(bf16[4,8,128,256]{3,2,1,0:T(8,128)(2,1)} %bitcast.54), calls=%async_computation.2 | async-start | bytes 4194304 | tf_op jit(solution)/shard_map/all_to_all | solution.py:89
  30.1 3.6 %copy-start.17 = (bf16[2048,256]{1,0:T(8,128)(2,1)S(1)}, bf16[2048,256]{1,0:T(8,128)(2,1)}, u32[]{:S(2)}) copy-start(bf16[2048,256]{1,0:T(8,128)(2,1)} %param.26) | copy-start | bytes 3145732
  30.1 0.6 copy-start.8
  53.6 4.8 %copy-start.13 = (s32[4,4]{1,0:T(4,128)S(1)}, s32[4,4]{1,0:T(4,128)}, u32[]{:S(2)}) copy-start(s32[4,4]{1,0:T(4,128)} %param.27) | copy-start | bytes 196
  53.6 5.5 %copy-start.9 = (f32[256,2]{0,1:T(2,128)S(1)}, f32[256,2]{0,1:T(2,128)}, u32[]{:S(2)}) copy-start(f32[256,2]{0,1:T(2,128)} %copy-done.8) | copy-start | bytes 6148
  53.6 6.3 %copy-start.7 = (bf16[256,256]{1,0:T(8,128)(2,1)S(1)}, bf16[256,256]{1,0:T(8,128)(2,1)}, u32[]{:S(2)}) copy-start(bf16[256,256]{1,0:T(8,128)(2,1)} %convolution_convert_fusion.2) | copy-start | bytes 393220
  53.6 30.3 %all-to-all-start.1 = ((bf16[4,8,128,256]{3,2,1,0:T(8,128)(2,1)}), bf16[4,8,128,256]{3,2,1,0:T(8,128)(2,1)}, u32[]{:S(2)}, u32[]{:S(2)}) async-start(bf16[4,8,128,256]{3,2,1,0:T(8,128)(2,1)} %bitcast.53), calls=%async_computation.1 | async-start | bytes 4194304 | tf_op jit(solution)/shard_map/all_to_all | solution.py:90
  58.1 69.3 %reduce-scatter.2.cloned.1.call-start = ((), (), s32[]{:S(2)}) async-start(), calls=%async_computation.4 | async-start | bytes 1310720 | tf_op jit(solution)/shard_map/reduce_scatter | solution.py:110
  67.4 3.4 %copy-start.6 = (bf16[4,64,2,128]{3,2,1,0:T(2,128)(2,1)S(1)}, bf16[4,64,2,128]{3,2,1,0:T(2,128)(2,1)}, u32[]{:S(2)}) copy-start(bf16[4,64,2,128]{3,2,1,0:T(2,128)(2,1)} %reshape.285) | copy-start | bytes 393220
  72.5 1.0 copy-start.3
  87.2 3.1 %copy-start.5 = (bf16[256,2048]{1,0:T(8,128)(2,1)S(1)}, bf16[256,2048]{1,0:T(8,128)(2,1)}, u32[]{:S(2)}) copy-start(bf16[256,2048]{1,0:T(8,128)(2,1)} %param.15) | copy-start | bytes 3145732
  87.2 3.2 %copy-start.12 = (f32[2048]{0:T(1024)S(1)}, f32[2048]{0:T(1024)}, u32[]{:S(2)}) copy-start(f32[2048]{0:T(1024)} %param.16) | copy-start | bytes 24580
  87.2 3.2 %copy-start.15 = (f32[256]{0:T(256)S(1)}, f32[256]{0:T(256)}, u32[]{:S(2)}) copy-start(f32[256]{0:T(256)} %copy-done.14) | copy-start | bytes 3076
Sparse Core Ops, SparseCore 0:
  99.4 27.9 reduce-scatter.1
where the time goes:
time: 135 us; the launch traced here: 134 us
  waiting for transfers between devices  52.6 us (39%)
  matrix products  26.8 us (20%)
  local copies, waits for them, and re-layouts  19 us (14%)
  between operations  13.7 us (10%)
  starting transfers between devices  13.6 us (10%)
  other arithmetic  8.58 us (6%)
    reduce_scatter x1, waiting for transfers between devices, local(): lax.psum_scatter((jnp.dot(out_mix, w_out_mix, preferred_element_type=jnp....  28.1 us
    all_to_all x1, waiting for transfers between devices, local(): lax.all_to_all(key_store[wanted], 'st', split_axis=0, concat_axis=0, tile...  14.3 us
    all_to_all x1, waiting for transfers between devices, local(): lax.all_to_all(value_store[wanted], 'st', split_axis=0, concat_axis=0, ti...  10.1 us
    reduce_sum x2, other arithmetic, row_norm(): jnp.mean(widened * widened, axis=-1, keepdims=True) + eps  4.73 us
    dot_general x1, matrix products, local(): jnp.dot(out_mix, w_out_mix, preferred_element_type=jnp.float32)  4.61 us
    all_to_all x1, starting transfers between devices, local(): lax.all_to_all(value_store[wanted], 'st', split_axis=0, concat_axis=0, ti...  4.58 us
    all_to_all x1, starting transfers between devices, local(): lax.all_to_all(key_store[wanted], 'st', split_axis=0, concat_axis=0, tile...  4.58 us
    all_to_all x1, starting transfers between devices, local(): lax.all_to_all(table, 'st', split_axis=0, concat_axis=0, tiled=True)  4.26 us
  transfers between devices with their start and end apart: 4, of which 3 were waited for; matrix products, arithmetic and copies ran while one was open for 24% of the time, Pallas kernels for 0%

commit v1 on v0

v1 whole, which is shorter than its diff:
```python
import functools

import jax
import jax.numpy as jnp
from jax import lax
from jax.experimental import pallas as pl
from jax.experimental.pallas import tpu as pltpu
from jax.sharding import PartitionSpec as P

HD = 128
SPAN = 128
RBLOCK = 64
PROWS = 128
FAR = -1e30
STAT_ROWS = 16

eps = 1e-06
f32 = jnp.float32
bf16 = jnp.bfloat16


def row_norm(values_in, gain):
    widened = values_in.astype(f32)
    return (
        widened * lax.rsqrt(jnp.mean(widened * widened, axis=-1, keepdims=True) + eps) * gain
    ).astype(bf16)


def pieces_of(row):
    high = row.astype(bf16).astype(f32)
    rest = row - high
    mid = rest.astype(bf16).astype(f32)
    low = (rest - mid).astype(bf16).astype(f32)
    return high, mid, low


def attend_kernel(ids_ref, q_ref, k_ref, v_ref, out_ref, *, held):
    rows, width = q_ref.shape
    base = lax.axis_index("st") * held
    passage = lax.broadcasted_iota(jnp.int32, (held, rows), 0)
    block = lax.broadcasted_iota(jnp.int32, (held, rows), 1) // RBLOCK
    count = jnp.zeros((held, rows), f32)
    for b in range(ids_ref.shape[0]):
        for j in range(ids_ref.shape[1]):
            hit = (passage == ids_ref[b, j] - base) & (block == b)
            count = count + jnp.where(hit, 1.0, 0.0)
    bias = jnp.where(count > 0.0, jnp.log(jnp.maximum(count, 1.0)), FAR)
    which = lax.broadcasted_iota(jnp.int32, (STAT_ROWS, rows), 0)
    stats = jnp.zeros((STAT_ROWS, rows), f32)
    for h in range(width // HD):
        cols = slice(h * HD, (h + 1) * HD)
        scores = lax.dot_general(
            k_ref[:, cols], q_ref[:, cols], (((1,), (1,)), ((), ())), preferred_element_type=f32
        ) * HD ** (-0.5)
        shifted = scores.reshape(held, PROWS, rows) + bias[:, None, :]
        top = jnp.max(jnp.max(shifted, axis=0), axis=0, keepdims=True)
        weights = jnp.exp(shifted - top[None])
        total = jnp.sum(jnp.sum(weights, axis=0), axis=0, keepdims=True)
        read = lax.dot_general(
            weights.astype(bf16).reshape(held * PROWS, rows),
            v_ref[:, cols],
            (((0,), (0,)), ((), ())),
            preferred_element_type=f32,
        )
        out_ref[:rows, cols] = read.astype(bf16)
        for i, piece in enumerate(pieces_of(top) + pieces_of(total)):
            stats = jnp.where(which == h * 6 + i, piece, stats)
    if rows == width:
        out_ref[rows:, :] = stats.astype(bf16)
    else:
        for part in range(rows // width):
            start = rows + part * STAT_ROWS
            out_ref[start : start + STAT_ROWS, :] = stats[:, part * width : (part + 1) * width].astype(bf16)


def attend(ids, query, keys, values, held):
    rows, width = query.shape
    return pl.pallas_call(
        functools.partial(attend_kernel, held=held),
        out_shape=jax.ShapeDtypeStruct((rows + STAT_ROWS * (rows // width), width), bf16),
        in_specs=[pl.BlockSpec(memory_space=pltpu.SMEM)] + [pl.BlockSpec(memory_space=pltpu.VMEM)] * 3,
        out_specs=pl.BlockSpec(memory_space=pltpu.VMEM),
        cost_estimate=pl.CostEstimate(
            flops=4 * rows * keys.shape[0] * width,
            transcendentals=rows * keys.shape[0] * (width // HD),
            bytes_accessed=2 * (2 * keys.size + 2 * query.size),
        ),
        name="attend",
    )(ids, query, keys, values)


def mix_kernel(mixed_ref, gated_ref, gate_ref, mixw_ref, out_ref):
    rows, width = mixed_ref.shape
    groups = mixw_ref.shape[0]
    group_width = width // groups
    mixed = mixed_ref[...]
    lane = lax.broadcasted_iota(jnp.int32, (1, width), 1) // group_width
    inside = [lane == g for g in range(groups)]

    def group_mean(value):
        result = jnp.zeros_like(value)
        for g in range(groups):
            mean = jnp.sum(jnp.where(inside[g], value, 0.0), axis=-1, keepdims=True) / group_width
            result = jnp.where(inside[g], mean, result)
        return result

    centred = mixed - group_mean(mixed)
    normal = (centred * lax.rsqrt(group_mean(centred * centred) + eps)).astype(bf16)
    below = lax.broadcasted_iota(jnp.int32, (SPAN, SPAN), 0) >= lax.broadcasted_iota(
        jnp.int32, (SPAN, SPAN), 1
    )
    masked = [jnp.where(below, mixw_ref[g].astype(f32), 0.0).astype(bf16) for g in range(groups)]
    for n in range(rows // SPAN):
        part = slice(n * SPAN, (n + 1) * SPAN)
        spatial = jnp.zeros((SPAN, width), f32)
        for g in range(groups):
            spatial = jnp.where(
                inside[g], jnp.dot(masked[g], normal[part], preferred_element_type=f32), spatial
            )
        gate = gate_ref[part, :]
        out_ref[part, :] = (gated_ref[part, :] * spatial * (gate / (1.0 + jnp.exp(-gate)))).astype(bf16)


def mix(mixed_in, gated, gate_mix, mix_weight):
    return pl.pallas_call(
        mix_kernel,
        out_shape=jax.ShapeDtypeStruct(mixed_in.shape, bf16),
        in_specs=[pl.BlockSpec(memory_space=pltpu.VMEM)] * 4,
        out_specs=pl.BlockSpec(memory_space=pltpu.VMEM),
        cost_estimate=pl.CostEstimate(
            flops=2 * mixed_in.size * SPAN * mix_weight.shape[0] + 20 * mixed_in.size,
            transcendentals=mixed_in.size,
            bytes_accessed=14 * mixed_in.size,
        ),
        name="mix",
    )(mixed_in, gated, gate_mix, mix_weight)


def finish_kernel(*refs, owners, shares):
    parts = refs[:owners]
    gate_ref, mix_ref, w_mix_ref, w_read_ref = refs[owners : owners + 4]
    outs = refs[owners + 4 : owners + 4 + shares]
    whole_ref = refs[owners + 4 + shares]
    rows, width = gate_ref.shape
    heads = width // HD
    stats = []
    for part in parts:
        pieces = [
            part[rows + i * STAT_ROWS : rows + (i + 1) * STAT_ROWS, :].astype(f32)
            for i in range(rows // width)
        ]
        stats.append(pieces[0] if len(pieces) == 1 else jnp.concatenate(pieces, axis=1))

    def value_of(stat, row):
        return stat[row : row + 1] + stat[row + 1 : row + 2] + stat[row + 2 : row + 3]

    for h in range(heads):
        cols = slice(h * HD, (h + 1) * HD)
        tops = [value_of(stat, h * 6) for stat in stats]
        highest = functools.reduce(jnp.maximum, tops)
        scales = [jnp.exp(top - highest) for top in tops]
        total = sum(scale * value_of(stat, h * 6 + 3) for scale, stat in zip(scales, stats))
        shares_of = [scale / total for scale in scales]
        padding = (-len(shares_of)) % 8
        square = jnp.concatenate(shares_of + [jnp.zeros((padding, rows), f32)] * (padding > 0), axis=0)
        columns = jnp.transpose(square)
        read = jnp.zeros((rows, HD), f32)
        for i, part in enumerate(parts):
            read = read + columns[:, i : i + 1] * part[:rows, cols].astype(f32)
        gate = gate_ref[:, cols]
        gated = (read * (gate / (1.0 + jnp.exp(-gate)))).astype(bf16)
        if h == 0:
            total_read = [gated]
        else:
            total_read.append(gated)
    out_read = total_read[0] if heads == 1 else jnp.concatenate(total_read, axis=1)
    partial = jnp.dot(mix_ref[...], w_mix_ref[...], preferred_element_type=f32) + jnp.dot(
        out_read, w_read_ref[...], preferred_element_type=f32
    )
    whole_ref[...] = partial.astype(bf16)
    here = lax.axis_index("tp")
    share_rows = rows // shares
    for k in range(shares):
        start = pl.multiple_of(((here + k) % shares) * share_rows, share_rows)
        outs[k][...] = whole_ref[pl.ds(start, share_rows), :]


def finish(parts, gate_read, out_mix, w_out_mix, w_out_read, shares):
    rows = gate_read.shape[0]
    model = w_out_mix.shape[1]
    share = jax.ShapeDtypeStruct((rows // shares, model), bf16)
    return pl.pallas_call(
        functools.partial(finish_kernel, owners=len(parts), shares=shares),
        out_shape=[share] * shares,
        in_specs=[pl.BlockSpec(memory_space=pltpu.VMEM)] * (len(parts) + 4),
        out_specs=[pl.BlockSpec(memory_space=pltpu.VMEM)] * shares,
        scratch_shapes=[pltpu.VMEM((rows, model), bf16)],
        cost_estimate=pl.CostEstimate(
            flops=2 * rows * model * (w_out_mix.shape[0] + w_out_read.shape[0]),
            transcendentals=gate_read.size,
            bytes_accessed=2 * (w_out_mix.size + w_out_read.size + rows * model),
        ),
        name="finish",
    )(*parts, gate_read, out_mix, w_out_mix, w_out_read)


def shifted_by(value, axis, step):
    count = lax.axis_size(axis)
    if step % count == 0:
        return value
    return lax.ppermute(value, axis, [(i, (i + step) % count) for i in range(count)])


def local(
    tokens,
    pre_gain,
    w_gated,
    w_mixed,
    mix_weight,
    w_query,
    w_gate_mix,
    w_gate_read,
    store,
    mem_gain,
    w_key,
    w_value,
    passage_ids,
    w_out_mix,
    w_out_read,
):
    readers = lax.axis_size("st")
    shares = lax.axis_size("tp")
    held = store.shape[0]
    ids = [shifted_by(passage_ids, "st", k) for k in range(readers)]
    normed = lax.optimization_barrier(row_norm(tokens, pre_gain))
    query = jnp.dot(normed, w_query, preferred_element_type=f32).astype(bf16)
    queries = [shifted_by(query, "st", k) for k in range(readers)]
    held_rows = lax.optimization_barrier(row_norm(store, mem_gain).reshape(-1, store.shape[-1]))
    keys = jnp.dot(held_rows, w_key, preferred_element_type=f32).astype(bf16)
    values = jnp.dot(held_rows, w_value, preferred_element_type=f32).astype(bf16)
    parts = [None] * readers
    for k in list(range(1, readers)) + [0]:
        parts[k] = shifted_by(attend(ids[k], queries[k], keys, values, held), "st", -k)
    gated = jnp.dot(normed, w_gated, preferred_element_type=f32)
    mixed_in = jnp.dot(normed, w_mixed, preferred_element_type=f32)
    gate_mix = jnp.dot(normed, w_gate_mix, preferred_element_type=f32)
    gate_read = jnp.dot(normed, w_gate_read, preferred_element_type=f32)
    out_mix = mix(mixed_in, gated, gate_mix, mix_weight)
    chunks = finish(parts, gate_read, out_mix, w_out_mix, w_out_read, shares)
    arrived = [shifted_by(chunks[k], "tp", k) for k in range(shares)]
    return functools.reduce(jnp.add, [part.astype(f32) for part in arrived]).astype(bf16)


def solution(mesh):
    placed = (
        P(("grp", "st"), None),
        P(),
        P(None, "tp"),
        P(None, "tp"),
        P("tp", None, None),
        P(None, "tp"),
        P(None, "tp"),
        P(None, "tp"),
        P(("grp", "st"), None, None),
        P(),
        P(None, "tp"),
        P(None, "tp"),
        P(("grp", "st"), None),
        P("tp", None),
        P("tp", None),
    )
    return jax.shard_map(
        local, mesh=mesh, in_specs=placed, out_specs=P(("grp", "st", "tp"), None), check_vma=False
    )
```

time: 135 us -> 79.8 us (0.59)
  the two profiles are of different devices: /device:TPU:0 before, /device:TPU:9 now
where the time goes in v1:
time: 79.8 us; the launch traced here: 79.4 us
  waiting for transfers between devices  22.5 us (28%)
  Pallas kernels  22.1 us (28%)
  starting transfers between devices  11.8 us (15%)
  matrix products  11.3 us (14%)
  other arithmetic  6.9 us (9%)
  local copies, waits for them, and re-layouts  4.69 us (6%)
    ppermute x12, waiting for transfers between devices, shifted_by(): lax.ppermute(value, axis, [(i, (i + step) % count) for i in range(count)])  22.5 us
    pallas_call x4, Pallas kernels, attend(): pl.pallas_call(functools.partial(attend_kernel, held=held), out_shape=jax...  14.9 us
    ppermute x12, starting transfers between devices, shifted_by(): lax.ppermute(value, axis, [(i, (i + step) % count) for i in range(count)])  11.8 us
    pallas_call x1, Pallas kernels, finish(): pl.pallas_call(functools.partial(finish_kernel, owners=len(parts), shares...  4.74 us
    unnamed x38, local copies, waits for them, and re-layouts  4.69 us
    convert_element_type x2, other arithmetic, row_norm(): return (widened * lax.rsqrt(jnp.mean(widened * widened, axis=-1, keepdims...  2.7 us
    pallas_call x1, Pallas kernels, mix(): pl.pallas_call(mix_kernel, out_shape=jax.ShapeDtypeStruct(mixed_in.shape,...  2.46 us
    reduce_sum x2, other arithmetic, row_norm(): jnp.mean(widened * widened, axis=-1, keepdims=True) + eps  2.39 us
  transfers between devices with their start and end apart: 12, of which 3 were waited for; matrix products, arithmetic and copies ran while one was open for 21% of the time, Pallas kernels for 22%

profile of v1, /device:TPU:9, one launch (start us, length us, event | category | flops | bytes accessed | tf_op | source)
XLA Modules:
  0.0 79.4 jit_solution(8075269493348925860)
XLA Ops:
  0.0 1.8 %collective-permute-start = (s32[4,4]{1,0:T(4,128)}, s32[4,4]{1,0:T(4,128)S(1)}, u32[]{:S(2)}, u32[]{:S(2)}) collective-permute-start(s32[4,4]{1,0:T(4,128)} %ids_ref.1), channel_id=1, source_target_pairs={{0,4},{4,8},{8,12},{12,0},{1,5},{5,9},{9,13},{13,1},{2,6},{6,10},{... | collective-permute-start | bytes 200 | tf_op jit(solution)/shard_map/ppermute | solution.py:211
  1.8 1.5 %fusion.3 = f32[256]{0:T(256)S(1)} fusion(bf16[256,2048]{1,0:T(8,128)(2,1)} %param.15), kind=kLoop, calls=%fused_computation.7 | loop fusion | flops 1572608 | bytes 1049600 | tf_op jit(solution)/shard_map/reduce_sum | solution.py:25
  3.3 1.7 %fusion.5 = bf16[256,2048]{1,0:T(8,128)(2,1)S(1)} fusion(bf16[256,2048]{1,0:T(8,128)(2,1)} %param.15, f32[2048]{0:T(1024)} %param.16, f32[256]{0:T(256)S(1)} %add_rsqrt_fusion.1), kind=kLoop, calls=%fused_computation.9 | loop fusion | flops 2097152 | bytes 2106368 | tf_op jit(solution)/shard_map/convert_element_type | solution.py:26
  5.5 0.7 collective-permute-start.7
  6.2 1.2 %collective-permute-start.4 = (bf16[256,256]{1,0:T(8,128)(2,1)S(1)}, bf16[256,256]{1,0:T(8,128)(2,1)S(1)}, u32[]{:S(2)}, u32[]{:S(2)}) collective-permute-start(bf16[256,256]{1,0:T(8,128)(2,1)S(1)} %convolution_convert_fusion.2.q_ref), channel_id=1, source_target_pairs={{0,8},{4,12},{8,0},{12,4},{1,9},{5,13},{9,1},{13,5},{2,10},{6,14},... | collective-permute-start | bytes 393224 | tf_op jit(solution)/shard_map/ppermute | solution.py:211
  7.9 0.9 %fusion = f32[8,128]{1,0:T(8,128)S(1)} fusion(bf16[8,128,2048]{2,1,0:T(8,128)(2,1)S(1)} %copy-done.1), kind=kLoop, calls=%fused_computation.2 | loop fusion | flops 6290432 | bytes 4198400 | tf_op jit(solution)/shard_map/reduce_sum | solution.py:25
  8.8 1.5 %fusion.9.gate_ref = f32[256,384]{1,0:T(8,128)} fusion(bf16[256,2048]{1,0:T(8,128)(2,1)S(1)} %fusion.5, bf16[2048,384]{1,0:T(8,128)(2,1)S(1)} %copy-done), kind=kOutput, calls=%fused_computation.19 | convolution fusion | flops 402653184 | bytes 3014656 | tf_op jit(solution)/shard_map/dot_general | solution.py:246
  10.3 1.5 %fusion.8.gated_ref = f32[256,384]{1,0:T(8,128)} fusion(bf16[256,2048]{1,0:T(8,128)(2,1)S(1)} %fusion.5, bf16[2048,384]{1,0:T(8,128)(2,1)S(1)} %copy-done.2), kind=kOutput, calls=%fused_computation.18 | convolution fusion | flops 402653184 | bytes 3014656 | tf_op jit(solution)/shard_map/dot_general | solution.py:244
  11.7 1.0 %fusion.2 = bf16[8,128,2048]{2,1,0:T(8,128)(2,1)S(1)} fusion(bf16[8,128,2048]{2,1,0:T(8,128)(2,1)S(1)} %copy-done.1, f32[2048]{0:T(1024)S(1)} %copy-done.12, f32[8,128]{1,0:T(8,128)S(1)} %add_rsqrt_fusion), kind=kLoop, calls=%fused_computation.4 | loop fusion | flops 8388608 | bytes 8400896 | tf_op jit(solution)/shard_map/convert_element_type | solution.py:26
  13.0 2.1 %convolution_convert_fusion.v_ref = bf16[1024,256]{1,0:T(8,128)(2,1)} fusion(bf16[1024,2048]{1,0:T(8,128)(2,1)S(1)} %bitcast.15, bf16[2048,256]{1,0:T(8,128)(2,1)S(1)} %copy-done.17), kind=kOutput, calls=%fused_computation.10 | convolution fusion | flops 1074003968 | bytes 5767168 | tf_op jit(solution)/shard_map/dot_general | solution.py:240
  15.0 2.1 %convolution_convert_fusion.1.k_ref = bf16[1024,256]{1,0:T(8,128)(2,1)} fusion(bf16[1024,2048]{1,0:T(8,128)(2,1)S(1)} %bitcast.16, bf16[2048,256]{1,0:T(8,128)(2,1)S(1)} %copy-done.18), kind=kOutput, calls=%fused_computation.11 | convolution fusion | flops 1074003968 | bytes 5767168 | tf_op jit(solution)/shard_map/dot_general | solution.py:239
  17.1 1.5 %fusion.7.mixed_ref = f32[256,384]{1,0:T(8,128)} fusion(bf16[256,2048]{1,0:T(8,128)(2,1)S(1)} %fusion.5, bf16[2048,384]{1,0:T(8,128)(2,1)S(1)} %copy-done.3), kind=kOutput, calls=%fused_computation.17 | convolution fusion | flops 402653184 | bytes 3014656 | tf_op jit(solution)/shard_map/dot_general | solution.py:245
  18.6 1.3 %collective-permute-start.3 = (s32[4,4]{1,0:T(4,128)S(1)}, s32[4,4]{1,0:T(4,128)S(1)}, u32[]{:S(2)}, u32[]{:S(2)}) collective-permute-start(s32[4,4]{1,0:T(4,128)S(1)} %copy-done.13), channel_id=1, source_target_pairs={{0,8},{4,12},{8,0},{12,4},{1,9},{5,13},{9,1},{13,5},{2,10},{6,14},... | collective-permute-start | bytes 200 | tf_op jit(solution)/shard_map/ppermute | solution.py:211
  19.9 0.7 copy-done.11
  20.5 3.7 %attend.5 = bf16[272,256]{1,0:T(8,128)(2,1)} custom-call(s32[4,4]{1,0:T(4,128)} %copy-done.15, bf16[256,256]{1,0:T(8,128)(2,1)} %copy-done.11, bf16[1024,256]{1,0:T(8,128)(2,1)} %convolution_convert_fusion.1.k_ref, bf16[1024,256]{1,0:T(8,128)(2,1)} %convolution_convert_fusion.v_ref), custom_call_target="tpu_custom_call" | custom-call | flops 268435456 | bytes 1310720 | tf_op jit(solution)/shard_map/attend/pallas_call | solution.py:78
  24.8 0.7 copy-done.10
  25.5 3.7 %attend.6 = bf16[272,256]{1,0:T(8,128)(2,1)} custom-call(s32[4,4]{1,0:T(4,128)} %copy-done.16, bf16[256,256]{1,0:T(8,128)(2,1)} %copy-done.10, bf16[1024,256]{1,0:T(8,128)(2,1)} %convolution_convert_fusion.1.k_ref, bf16[1024,256]{1,0:T(8,128)(2,1)} %convolution_convert_fusion.v_ref), custom_call_target="tpu_custom_call" | custom-call | flops 268435456 | bytes 1310720 | tf_op jit(solution)/shard_map/attend/pallas_call | solution.py:78
  30.4 0.7 copy-done.9
  31.0 3.7 %attend.7 = bf16[272,256]{1,0:T(8,128)(2,1)} custom-call(s32[4,4]{1,0:T(4,128)} %copy-done.14, bf16[256,256]{1,0:T(8,128)(2,1)} %copy-done.9, bf16[1024,256]{1,0:T(8,128)(2,1)} %convolution_convert_fusion.1.k_ref, bf16[1024,256]{1,0:T(8,128)(2,1)} %convolution_convert_fusion.v_ref), custom_call_target="tpu_custom_call" | custom-call | flops 268435456 | bytes 1310720 | tf_op jit(solution)/shard_map/attend/pallas_call | solution.py:78
  34.7 2.0 %collective-permute-start.8 = (bf16[272,256]{1,0:T(8,128)(2,1)}, bf16[272,256]{1,0:T(8,128)(2,1)S(1)}, u32[]{:S(2)}, u32[]{:S(2)}) collective-permute-start(bf16[272,256]{1,0:T(8,128)(2,1)} %attend.7), channel_id=1, source_target_pairs={{0,4},{4,8},{8,12},{12,0},{1,5},{5,9},{9,13},{13,1},{2,6},{6,10},{... | collective-permute-start | bytes 417800 | tf_op jit(solution)/shard_map/ppermute | solution.py:211
  36.7 2.4 %fusion.6.refs_4_ = f32[256,256]{1,0:T(8,128)} fusion(bf16[256,2048]{1,0:T(8,128)(2,1)S(1)} %fusion.5, bf16[2048,256]{1,0:T(8,128)(2,1)} %param.22), kind=kOutput, calls=%fused_computation.16 | convolution fusion | flops 268435456 | bytes 2359296 | tf_op jit(solution)/shard_map/dot_general | solution.py:247
  39.1 2.5 %mix.1.refs_5_ = bf16[256,384]{1,0:T(8,128)(2,1)} custom-call(f32[256,384]{1,0:T(8,128)} %fusion.7.mixed_ref, f32[256,384]{1,0:T(8,128)} %fusion.8.gated_ref, f32[256,384]{1,0:T(8,128)} %fusion.9.gate_ref, bf16[2,128,128]{2,1,0:T(8,128)(2,1)} %mixw_ref.1), custom_call_target="tpu_custom_call" | custom-call | flops 52297728 | bytes 1376256 | tf_op jit(solution)/shard_map/mix/pallas_call | solution.py:125
  41.5 3.7 %attend.4.refs_0_ = bf16[272,256]{1,0:T(8,128)(2,1)} custom-call(s32[4,4]{1,0:T(4,128)} %ids_ref.1, bf16[256,256]{1,0:T(8,128)(2,1)} %copy-done.5, bf16[1024,256]{1,0:T(8,128)(2,1)} %convolution_convert_fusion.1.k_ref, bf16[1024,256]{1,0:T(8,128)(2,1)} %convolution_convert_fusion.v_ref), custom_call_target="tpu_custom_call" | custom-call | flops 268435456 | bytes 1310720 | tf_op jit(solution)/shard_map/attend/pallas_call | solution.py:78
  46.0 0.7 copy-done.8
  46.6 4.7 %finish.1 = (bf16[64,2048]{1,0:T(8,128)(2,1)}, bf16[64,2048]{1,0:T(8,128)(2,1)}, bf16[64,2048]{1,0:T(8,128)(2,1)}, bf16[64,2048]{1,0:T(8,128)(2,1)}) custom-call(bf16[272,256]{1,0:T(8,128)(2,1)} %attend.4.refs_0_, bf16[272,256]{1,0:T(8,128)(2,1)} %copy-done.6, bf16[272,256]{1,0:T(8,128)(2,1)} %copy-done.7, bf16[272,256]{1,0:T(8,128)(2,1)} %copy-done.8, ...), custom_call_target="tpu_custom_call" | custom-call | flops 671088640 | bytes 3670016 | tf_op jit(solution)/shard_map/finish/pallas_call | solution.py:192
  51.4 1.3 %collective-permute-start.9 = (bf16[64,2048]{1,0:T(8,128)(2,1)}, bf16[64,2048]{1,0:T(8,128)(2,1)S(1)}, u32[]{:S(2)}, u32[]{:S(2)}) collective-permute-start(bf16[64,2048]{1,0:T(8,128)(2,1)} %get-tuple-element.10), channel_id=1, source_target_pairs={{0,1},{1,2},{2,3},{3,0},{4,5},{5,6},{6,7},{7,4},{8,9},{9,10},{10,1... | collective-permute-start | bytes 786440 | tf_op jit(solution)/shard_map/ppermute | solution.py:211
  52.7 1.0 %collective-permute-start.10 = (bf16[64,2048]{1,0:T(8,128)(2,1)}, bf16[64,2048]{1,0:T(8,128)(2,1)S(1)}, u32[]{:S(2)}, u32[]{:S(2)}) collective-permute-start(bf16[64,2048]{1,0:T(8,128)(2,1)} %get-tuple-element.11), channel_id=1, source_target_pairs={{0,2},{1,3},{2,0},{3,1},{4,6},{5,7},{6,4},{7,5},{8,10},{9,11},{10,... | collective-permute-start | bytes 786440 | tf_op jit(solution)/shard_map/ppermute | solution.py:211
  53.7 1.5 %collective-permute-start.11 = (bf16[64,2048]{1,0:T(8,128)(2,1)}, bf16[64,2048]{1,0:T(8,128)(2,1)S(1)}, u32[]{:S(2)}, u32[]{:S(2)}) collective-permute-start(bf16[64,2048]{1,0:T(8,128)(2,1)} %get-tuple-element.12), channel_id=1, source_target_pairs={{0,3},{1,0},{2,1},{3,2},{4,7},{5,4},{6,5},{7,6},{8,11},{9,8},{10,9... | collective-permute-start | bytes 786440 | tf_op jit(solution)/shard_map/ppermute | solution.py:211
  55.2 4.7 %collective-permute-done.9 = bf16[64,2048]{1,0:T(8,128)(2,1)S(1)} collective-permute-done((bf16[64,2048]{1,0:T(8,128)(2,1)}, bf16[64,2048]{1,0:T(8,128)(2,1)S(1)}, u32[]{:S(2)}, u32[]{:S(2)}) %collective-permute-start.9) | collective-permute-done | bytes 262176 | tf_op jit(solution)/shard_map/ppermute | solution.py:211
  59.8 16.1 %collective-permute-done.10 = bf16[64,2048]{1,0:T(8,128)(2,1)S(1)} collective-permute-done((bf16[64,2048]{1,0:T(8,128)(2,1)}, bf16[64,2048]{1,0:T(8,128)(2,1)S(1)}, u32[]{:S(2)}, u32[]{:S(2)}) %collective-permute-start.10) | collective-permute-done | bytes 262176 | tf_op jit(solution)/shard_map/ppermute | solution.py:211
  75.9 1.7 %collective-permute-done.11 = bf16[64,2048]{1,0:T(8,128)(2,1)S(1)} collective-permute-done((bf16[64,2048]{1,0:T(8,128)(2,1)}, bf16[64,2048]{1,0:T(8,128)(2,1)S(1)}, u32[]{:S(2)}, u32[]{:S(2)}) %collective-permute-start.11) | collective-permute-done | bytes 262176 | tf_op jit(solution)/shard_map/ppermute | solution.py:211
  77.6 1.8 %add_convert_fusion = bf16[64,2048]{1,0:T(8,128)(2,1)} fusion(bf16[64,2048]{1,0:T(8,128)(2,1)S(1)} %collective-permute-done.11, bf16[64,2048]{1,0:T(8,128)(2,1)S(1)} %collective-permute-done.10, bf16[64,2048]{1,0:T(8,128)(2,1)S(1)} %collective-permute-done.9, bf16[64,2048]{1,0:T(8,128)(2,1)} %get-tuple-element.9), kind=kLoop, calls=%fused_computation.13 | loop fusion | flops 1048576 | bytes 1310720 | tf_op jit(solution)/shard_map/convert_element_type | solution.py:251
  (50 shorter events, 3.6 us)
Async XLA Ops:
  0.0 8.8 %copy-start = (bf16[2048,384]{1,0:T(8,128)(2,1)S(1)}, bf16[2048,384]{1,0:T(8,128)(2,1)}, u32[]{:S(2)}) copy-start(bf16[2048,384]{1,0:T(8,128)(2,1)} %param.21) | copy-start | bytes 4718596
  0.0 5.0 %copy-start.4 = (bf16[2048,256]{1,0:T(8,128)(2,1)S(1)}, bf16[2048,256]{1,0:T(8,128)(2,1)}, u32[]{:S(2)}) copy-start(bf16[2048,256]{1,0:T(8,128)(2,1)} %param.20) | copy-start | bytes 3145732
  0.0 18.6 %collective-permute-start = (s32[4,4]{1,0:T(4,128)}, s32[4,4]{1,0:T(4,128)S(1)}, u32[]{:S(2)}, u32[]{:S(2)}) collective-permute-start(s32[4,4]{1,0:T(4,128)} %ids_ref.1), channel_id=1, source_target_pairs={{0,4},{4,8},{8,12},{12,0},{1,5},{5,9},{9,13},{13,1},{2,6},{6,10},{... | collective-permute-start | bytes 200 | tf_op jit(solution)/shard_map/ppermute | solution.py:211
  1.8 28.0 %collective-permute-start.6 = (s32[4,4]{1,0:T(4,128)}, s32[4,4]{1,0:T(4,128)S(1)}, u32[]{:S(2)}, u32[]{:S(2)}) collective-permute-start(s32[4,4]{1,0:T(4,128)} %ids_ref.1), channel_id=1, source_target_pairs={{0,12},{4,0},{8,4},{12,8},{1,13},{5,1},{9,5},{13,9},{2,14},{6,2},{... | collective-permute-start | bytes 200 | tf_op jit(solution)/shard_map/ppermute | solution.py:211
  3.3 4.6 %copy-start.1 = (bf16[8,128,2048]{2,1,0:T(8,128)(2,1)S(1)}, bf16[8,128,2048]{2,1,0:T(8,128)(2,1)}, u32[]{:S(2)}) copy-start(bf16[8,128,2048]{2,1,0:T(8,128)(2,1)} %param.23) | copy-start | bytes 12582916
  5.5 3.3 %copy-start.5 = (bf16[256,256]{1,0:T(8,128)(2,1)}, bf16[256,256]{1,0:T(8,128)(2,1)S(1)}, u32[]{:S(2)}) copy-start(bf16[256,256]{1,0:T(8,128)(2,1)S(1)} %convolution_convert_fusion.2.q_ref) | copy-start | bytes 393220
  5.5 24.3 %collective-permute-start.7 = (bf16[256,256]{1,0:T(8,128)(2,1)S(1)}, bf16[256,256]{1,0:T(8,128)(2,1)S(1)}, u32[]{:S(2)}, u32[]{:S(2)}) collective-permute-start(bf16[256,256]{1,0:T(8,128)(2,1)S(1)} %convolution_convert_fusion.2.q_ref), channel_id=1, source_target_pairs={{0,12},{4,0},{8,4},{12,8},{1,13},{5,1},{9,5},{13,9},{2,14},{6,2},{... | collective-permute-start | bytes 393224 | tf_op jit(solution)/shard_map/ppermute | solution.py:211
  6.2 18.1 %collective-permute-start.4 = (bf16[256,256]{1,0:T(8,128)(2,1)S(1)}, bf16[256,256]{1,0:T(8,128)(2,1)S(1)}, u32[]{:S(2)}, u32[]{:S(2)}) collective-permute-start(bf16[256,256]{1,0:T(8,128)(2,1)S(1)} %convolution_convert_fusion.2.q_ref), channel_id=1, source_target_pairs={{0,8},{4,12},{8,0},{12,4},{1,9},{5,13},{9,1},{13,5},{2,10},{6,14},... | collective-permute-start | bytes 393224 | tf_op jit(solution)/shard_map/ppermute | solution.py:211
  7.4 12.5 %collective-permute-start.1 = (bf16[256,256]{1,0:T(8,128)(2,1)S(1)}, bf16[256,256]{1,0:T(8,128)(2,1)S(1)}, u32[]{:S(2)}, u32[]{:S(2)}) collective-permute-start(bf16[256,256]{1,0:T(8,128)(2,1)S(1)} %convolution_convert_fusion.2.q_ref), channel_id=1, source_target_pairs={{0,4},{4,8},{8,12},{12,0},{1,5},{5,9},{9,13},{13,1},{2,6},{6,10},{... | collective-permute-start | bytes 393224 | tf_op jit(solution)/shard_map/ppermute | solution.py:211
  8.8 1.5 %copy-start.2 = (bf16[2048,384]{1,0:T(8,128)(2,1)S(1)}, bf16[2048,384]{1,0:T(8,128)(2,1)}, u32[]{:S(2)}) copy-start(bf16[2048,384]{1,0:T(8,128)(2,1)} %param.17) | copy-start | bytes 4718596
  10.3 1.5 %copy-start.12 = (f32[2048]{0:T(1024)S(1)}, f32[2048]{0:T(1024)}, u32[]{:S(2)}) copy-start(f32[2048]{0:T(1024)} %param.24) | copy-start | bytes 24580
  11.7 1.2 %copy-start.17 = (bf16[2048,256]{1,0:T(8,128)(2,1)S(1)}, bf16[2048,256]{1,0:T(8,128)(2,1)}, u32[]{:S(2)}) copy-start(bf16[2048,256]{1,0:T(8,128)(2,1)} %param.26) | copy-start | bytes 3145732
  13.0 2.1 %copy-start.18 = (bf16[2048,256]{1,0:T(8,128)(2,1)S(1)}, bf16[2048,256]{1,0:T(8,128)(2,1)}, u32[]{:S(2)}) copy-start(bf16[2048,256]{1,0:T(8,128)(2,1)} %param.25) | copy-start | bytes 3145732
  15.0 2.1 %copy-start.3 = (bf16[2048,384]{1,0:T(8,128)(2,1)S(1)}, bf16[2048,384]{1,0:T(8,128)(2,1)}, u32[]{:S(2)}) copy-start(bf16[2048,384]{1,0:T(8,128)(2,1)} %param.18) | copy-start | bytes 4718596
  17.1 1.5 %copy-start.13 = (s32[4,4]{1,0:T(4,128)S(1)}, s32[4,4]{1,0:T(4,128)}, u32[]{:S(2)}) copy-start(s32[4,4]{1,0:T(4,128)} %ids_ref.1) | copy-start | bytes 196
  18.6 1.3 %copy-start.15 = (s32[4,4]{1,0:T(4,128)}, s32[4,4]{1,0:T(4,128)S(1)}, u32[]{:S(2)}) copy-start(s32[4,4]{1,0:T(4,128)S(1)} %collective-permute-done.ids_ref) | copy-start | bytes 196
  18.6 5.7 %collective-permute-start.3 = (s32[4,4]{1,0:T(4,128)S(1)}, s32[4,4]{1,0:T(4,128)S(1)}, u32[]{:S(2)}, u32[]{:S(2)}) collective-permute-start(s32[4,4]{1,0:T(4,128)S(1)} %copy-done.13), channel_id=1, source_target_pairs={{0,8},{4,12},{8,0},{12,4},{1,9},{5,13},{9,1},{13,5},{2,10},{6,14},... | collective-permute-start | bytes 200 | tf_op jit(solution)/shard_map/ppermute | solution.py:211
  19.9 0.7 copy-start.11
  24.3 21.0 %collective-permute-start.2 = (bf16[272,256]{1,0:T(8,128)(2,1)}, bf16[272,256]{1,0:T(8,128)(2,1)S(1)}, u32[]{:S(2)}, u32[]{:S(2)}) collective-permute-start(bf16[272,256]{1,0:T(8,128)(2,1)} %attend.5), channel_id=1, source_target_pairs={{0,12},{4,0},{8,4},{12,8},{1,13},{5,1},{9,5},{13,9},{2,14},{6,2},{... | collective-permute-start | bytes 417800 | tf_op jit(solution)/shard_map/ppermute | solution.py:211
  24.3 0.6 copy-start.16
  24.8 0.7 copy-start.10
  29.2 16.0 %collective-permute-start.5 = (bf16[272,256]{1,0:T(8,128)(2,1)}, bf16[272,256]{1,0:T(8,128)(2,1)S(1)}, u32[]{:S(2)}, u32[]{:S(2)}) collective-permute-start(bf16[272,256]{1,0:T(8,128)(2,1)} %attend.6), channel_id=1, source_target_pairs={{0,8},{4,12},{8,0},{12,4},{1,9},{5,13},{9,1},{13,5},{2,10},{6,14},... | collective-permute-start | bytes 417800 | tf_op jit(solution)/shard_map/ppermute | solution.py:211
  29.8 0.6 copy-start.14
  30.4 0.7 copy-start.9
  34.7 10.5 %collective-permute-start.8 = (bf16[272,256]{1,0:T(8,128)(2,1)}, bf16[272,256]{1,0:T(8,128)(2,1)S(1)}, u32[]{:S(2)}, u32[]{:S(2)}) collective-permute-start(bf16[272,256]{1,0:T(8,128)(2,1)} %attend.7), channel_id=1, source_target_pairs={{0,4},{4,8},{8,12},{12,0},{1,5},{5,9},{9,13},{13,1},{2,6},{6,10},{... | collective-permute-start | bytes 417800 | tf_op jit(solution)/shard_map/ppermute | solution.py:211
  45.3 0.6 copy-start.6
  45.3 0.7 copy-start.7
  46.0 0.7 copy-start.8
  51.4 8.5 %collective-permute-start.9 = (bf16[64,2048]{1,0:T(8,128)(2,1)}, bf16[64,2048]{1,0:T(8,128)(2,1)S(1)}, u32[]{:S(2)}, u32[]{:S(2)}) collective-permute-start(bf16[64,2048]{1,0:T(8,128)(2,1)} %get-tuple-element.10), channel_id=1, source_target_pairs={{0,1},{1,2},{2,3},{3,0},{4,5},{5,6},{6,7},{7,4},{8,9},{9,10},{10,1... | collective-permute-start | bytes 786440 | tf_op jit(solution)/shard_map/ppermute | solution.py:211
  52.7 23.2 %collective-permute-start.10 = (bf16[64,2048]{1,0:T(8,128)(2,1)}, bf16[64,2048]{1,0:T(8,128)(2,1)S(1)}, u32[]{:S(2)}, u32[]{:S(2)}) collective-permute-start(bf16[64,2048]{1,0:T(8,128)(2,1)} %get-tuple-element.11), channel_id=1, source_target_pairs={{0,2},{1,3},{2,0},{3,1},{4,6},{5,7},{6,4},{7,5},{8,10},{9,11},{10,... | collective-permute-start | bytes 786440 | tf_op jit(solution)/shard_map/ppermute | solution.py:211
  53.7 23.9 %collective-permute-start.11 = (bf16[64,2048]{1,0:T(8,128)(2,1)}, bf16[64,2048]{1,0:T(8,128)(2,1)S(1)}, u32[]{:S(2)}, u32[]{:S(2)}) collective-permute-start(bf16[64,2048]{1,0:T(8,128)(2,1)} %get-tuple-element.12), channel_id=1, source_target_pairs={{0,3},{1,0},{2,1},{3,2},{4,7},{5,4},{6,5},{7,6},{8,11},{9,8},{10,9... | collective-permute-start | bytes 786440 | tf_op jit(solution)/shard_map/ppermute | solution.py:211

commit v2 on v1

v2 whole, which is shorter than its diff:
```python
import functools

import jax
import jax.numpy as jnp
from jax import lax
from jax.experimental import pallas as pl
from jax.experimental.pallas import tpu as pltpu
from jax.sharding import PartitionSpec as P

HD = 128
SPAN = 128
RBLOCK = 64
PROWS = 128
FAR = -1e30
EXTRA = 16
NPB = 4

eps = 1e-06
f32 = jnp.float32
bf16 = jnp.bfloat16


LOG2E = 1.4426950408889634


def row_norm(values_in, gain):
    widened = values_in.astype(f32)
    return (
        widened * lax.rsqrt(jnp.mean(widened * widened, axis=-1, keepdims=True) + eps) * gain
    ).astype(bf16)


def pieces_of(row):
    high = row.astype(bf16).astype(f32)
    rest = row - high
    mid = rest.astype(bf16).astype(f32)
    low = (rest - mid).astype(bf16).astype(f32)
    return high, mid, low


def silu(gate):
    return gate / (1.0 + jnp.exp(-gate))


def query_kernel(first_ref, ids_ref, tokens_ref, gain_ref, w_ref, normed_ref, query_ref, *, held):
    rows = tokens_ref.shape[0]
    normed = row_norm(tokens_ref[...], gain_ref[...])
    normed_ref[...] = normed
    query_ref[:rows, :] = jnp.dot(normed, w_ref[...], preferred_element_type=f32).astype(bf16)
    width = query_ref.shape[1]
    blocks = rows // RBLOCK
    first_block = ((pl.program_id(0) + first_ref[0]) % 2) * blocks
    block = lax.broadcasted_iota(jnp.int32, (EXTRA, width), 1) // RBLOCK
    line = lax.broadcasted_iota(jnp.int32, (EXTRA, width), 0)
    table = jnp.zeros((EXTRA, width), jnp.int32)
    for b in range(blocks):
        for j in range(ids_ref.shape[1]):
            name = ids_ref[first_block + b, j]
            table = jnp.where((block == b) & (line == 2 * j), name // held, table)
            table = jnp.where((block == b) & (line == 2 * j + 1), name % held, table)
    query_ref[rows:, :] = table.astype(f32).astype(bf16)


def make_queries(first, ids, tokens, gain, w_query, held):
    rows, model = tokens.shape
    width = w_query.shape[1]
    half = rows // 2
    return pl.pallas_call(
        functools.partial(query_kernel, held=held),
        grid_spec=pltpu.PrefetchScalarGridSpec(
            num_scalar_prefetch=2,
            grid=(2,),
            in_specs=[
                pl.BlockSpec((half, model), lambda i, first, ids: ((i + first[0]) % 2, 0)),
                pl.BlockSpec((1, model), lambda i, first, ids: (0, 0)),
                pl.BlockSpec((model, width), lambda i, first, ids: (0, 0)),
            ],
            out_specs=[
                pl.BlockSpec((half, model), lambda i, first, ids: (i, 0)),
                pl.BlockSpec((half + EXTRA, width), lambda i, first, ids: (i, 0)),
            ],
        ),
        out_shape=[
            jax.ShapeDtypeStruct((rows, model), bf16),
            jax.ShapeDtypeStruct((rows + 2 * EXTRA, width), bf16),
        ],
        cost_estimate=pl.CostEstimate(
            flops=2 * rows * model * width,
            transcendentals=rows,
            bytes_accessed=2 * (2 * tokens.size + w_query.size),
        ),
        name="queries",
    )(first, ids, tokens, gain.reshape(1, -1), w_query)


def attend_kernel(q_ref, k_ref, v_ref, out_ref, *, held, part):
    rows = out_ref.shape[0] - EXTRA
    width = out_ref.shape[1]
    start = part * (rows + EXTRA)
    here = lax.axis_index("st").astype(f32)
    table = q_ref[start + rows : start + rows + EXTRA, :rows].astype(f32)
    passage = lax.broadcasted_iota(jnp.int32, (held, rows), 0).astype(f32)
    count = jnp.zeros((held, rows), f32)
    for j in range(NPB):
        mine = table[2 * j : 2 * j + 1] == here
        hit = (passage == table[2 * j + 1 : 2 * j + 2]) & mine
        count = count + jnp.where(hit, 1.0, 0.0)
    bias = jnp.where(count > 0.0, jnp.log2(jnp.maximum(count, 1.0)), FAR)
    which = lax.broadcasted_iota(jnp.int32, (EXTRA, rows), 0)
    for h in range(width // HD):
        cols = slice(h * HD, (h + 1) * HD)
        scores = lax.dot_general(
            k_ref[:, cols],
            q_ref[start : start + rows, cols],
            (((1,), (1,)), ((), ())),
            preferred_element_type=f32,
        ) * (HD ** (-0.5) * LOG2E)
        shifted = scores.reshape(held, PROWS, rows) + bias[:, None, :]
        top = jnp.max(jnp.max(shifted, axis=0), axis=0, keepdims=True)
        weights = jnp.exp2(shifted - top[None])
        total = jnp.sum(jnp.sum(weights, axis=0), axis=0, keepdims=True)
        read = lax.dot_general(
            weights.astype(bf16).reshape(held * PROWS, rows),
            v_ref[:, cols],
            (((0,), (0,)), ((), ())),
            preferred_element_type=f32,
        )
        out_ref[:rows, cols] = read.astype(bf16)
        stats = jnp.zeros((EXTRA, rows), f32)
        for i, piece in enumerate(pieces_of(top) + pieces_of(total)):
            stats = jnp.where(which == i, piece, stats)
        out_ref[rows:, h * HD : h * HD + rows] = stats.astype(bf16)


def attend(query, keys, values, held, part):
    rows = query.shape[0] // 2 - EXTRA
    width = query.shape[1]
    assert rows == HD
    return pl.pallas_call(
        functools.partial(attend_kernel, held=held, part=part),
        out_shape=jax.ShapeDtypeStruct((rows + EXTRA, width), bf16),
        in_specs=[pl.BlockSpec(memory_space=pltpu.VMEM)] * 3,
        out_specs=pl.BlockSpec(memory_space=pltpu.VMEM),
        cost_estimate=pl.CostEstimate(
            flops=4 * rows * keys.shape[0] * width,
            transcendentals=rows * keys.shape[0] * (width // HD),
            bytes_accessed=2 * (2 * keys.size + 2 * query.size),
        ),
        name="attend",
    )(query, keys, values)


def mix_kernel(mixed_ref, gated_ref, gate_ref, mixw_ref, out_ref, *, part):
    rows, width = out_ref.shape
    groups = mixw_ref.shape[0]
    group_width = width // groups
    start = part * rows
    mixed = mixed_ref[start : start + rows, :]
    lane = lax.broadcasted_iota(jnp.int32, (1, width), 1) // group_width
    inside = [lane == g for g in range(groups)]

    def group_mean(value):
        result = jnp.zeros_like(value)
        for g in range(groups):
            mean = jnp.sum(jnp.where(inside[g], value, 0.0), axis=-1, keepdims=True) / group_width
            result = jnp.where(inside[g], mean, result)
        return result

    centred = mixed - group_mean(mixed)
    normal = (centred * lax.rsqrt(group_mean(centred * centred) + eps)).astype(bf16)
    below = lax.broadcasted_iota(jnp.int32, (SPAN, SPAN), 0) >= lax.broadcasted_iota(
        jnp.int32, (SPAN, SPAN), 1
    )
    masked = [jnp.where(below, mixw_ref[g].astype(f32), 0.0).astype(bf16) for g in range(groups)]
    for n in range(rows // SPAN):
        block = slice(n * SPAN, (n + 1) * SPAN)
        source = slice(start + n * SPAN, start + (n + 1) * SPAN)
        spatial = jnp.zeros((SPAN, width), f32)
        for g in range(groups):
            spatial = jnp.where(
                inside[g], jnp.dot(masked[g], normal[block], preferred_element_type=f32), spatial
            )
        out_ref[block, :] = (gated_ref[source, :] * spatial * silu(gate_ref[source, :])).astype(bf16)


def mix(mixed_in, gated, gate_mix, mix_weight, part):
    rows, width = mixed_in.shape
    return pl.pallas_call(
        functools.partial(mix_kernel, part=part),
        out_shape=jax.ShapeDtypeStruct((rows // 2, width), bf16),
        in_specs=[pl.BlockSpec(memory_space=pltpu.VMEM)] * 4,
        out_specs=pl.BlockSpec(memory_space=pltpu.VMEM),
        cost_estimate=pl.CostEstimate(
            flops=mixed_in.size * SPAN * mix_weight.shape[0] + 10 * mixed_in.size,
            transcendentals=mixed_in.size // 2,
            bytes_accessed=7 * mixed_in.size,
        ),
        name="mix",
    )(mixed_in, gated, gate_mix, mix_weight)


def finish_kernel(*refs, owners, shares, part):
    parts = refs[:owners]
    gate_ref, mix_ref, w_mix_ref, w_read_ref = refs[owners : owners + 4]
    outs = refs[owners + 4 : owners + 4 + shares]
    whole_ref = refs[owners + 4 + shares]
    rows = mix_ref.shape[0]
    width = gate_ref.shape[1]
    out_read = []
    for h in range(width // HD):
        cols = slice(h * HD, (h + 1) * HD)
        stats = [p[rows:, h * HD : h * HD + rows].astype(f32) for p in parts]
        tops = [stat[0:1] + stat[1:2] + stat[2:3] for stat in stats]
        totals = [stat[3:4] + stat[4:5] + stat[5:6] for stat in stats]
        highest = functools.reduce(jnp.maximum, tops)
        scales = [jnp.exp2(top - highest) for top in tops]
        whole = sum(scale * total for scale, total in zip(scales, totals))
        weights = [scale / whole for scale in scales]
        padding = (-len(weights)) % 8
        square = jnp.concatenate(weights + [jnp.zeros((padding, rows), f32)] * (padding > 0), axis=0)
        columns = jnp.transpose(square)
        read = jnp.zeros((rows, HD), f32)
        for i, p in enumerate(parts):
            read = read + columns[:, i : i + 1] * p[:rows, cols].astype(f32)
        out_read.append((read * silu(gate_ref[part * rows : (part + 1) * rows, cols])).astype(bf16))
    out_read = out_read[0] if len(out_read) == 1 else jnp.concatenate(out_read, axis=1)
    partial = jnp.dot(mix_ref[...], w_mix_ref[...], preferred_element_type=f32) + jnp.dot(
        out_read, w_read_ref[...], preferred_element_type=f32
    )
    whole_ref[...] = partial.astype(bf16)
    here = lax.axis_index("tp")
    share_rows = rows // shares
    for k in range(shares):
        start = pl.multiple_of((jnp.bitwise_xor(here, k) % shares) * share_rows, share_rows)
        outs[k][...] = whole_ref[pl.ds(start, share_rows), :]


def finish(parts, gate_read, out_mix, w_out_mix, w_out_read, shares, part):
    rows = out_mix.shape[0]
    model = w_out_mix.shape[1]
    share = jax.ShapeDtypeStruct((rows // shares, model), bf16)
    return pl.pallas_call(
        functools.partial(finish_kernel, owners=len(parts), shares=shares, part=part),
        out_shape=[share] * shares,
        in_specs=[pl.BlockSpec(memory_space=pltpu.VMEM)] * (len(parts) + 4),
        out_specs=[pl.BlockSpec(memory_space=pltpu.VMEM)] * shares,
        scratch_shapes=[pltpu.VMEM((rows, model), bf16)],
        cost_estimate=pl.CostEstimate(
            flops=2 * rows * model * (w_out_mix.shape[0] + w_out_read.shape[0]),
            transcendentals=gate_read.size,
            bytes_accessed=2 * (w_out_mix.size + w_out_read.size + rows * model),
        ),
        name="finish",
    )(*parts, gate_read, out_mix, w_out_mix, w_out_read)


def shifted_by(value, axis, step):
    count = lax.axis_size(axis)
    if step % count == 0:
        return value
    return lax.ppermute(value, axis, [(i, (i + step) % count) for i in range(count)])


def crossed_by(value, axis, mask):
    if mask == 0:
        return value
    return lax.ppermute(value, axis, [(i, i ^ mask) for i in range(lax.axis_size(axis))])


def local(
    tokens,
    pre_gain,
    w_gated,
    w_mixed,
    mix_weight,
    w_query,
    w_gate_mix,
    w_gate_read,
    store,
    mem_gain,
    w_key,
    w_value,
    passage_ids,
    w_out_mix,
    w_out_read,
):
    readers = lax.axis_size("st")
    near = lax.axis_size("tp") // 2
    held = store.shape[0]
    first = (1 - lax.axis_index("tp") // near).astype(jnp.int32).reshape(1)
    normed, query = make_queries(first, passage_ids, tokens, pre_gain, w_query, held)
    queries = [shifted_by(query, "st", k) for k in range(readers)]
    held_rows = lax.optimization_barrier(row_norm(store, mem_gain).reshape(-1, store.shape[-1]))
    keys = jnp.dot(held_rows, w_key, preferred_element_type=f32).astype(bf16)
    values = jnp.dot(held_rows, w_value, preferred_element_type=f32).astype(bf16)
    gated = jnp.dot(normed, w_gated, preferred_element_type=f32)
    mixed_in = jnp.dot(normed, w_mixed, preferred_element_type=f32)
    gate_mix = jnp.dot(normed, w_gate_mix, preferred_element_type=f32)
    gate_read = jnp.dot(normed, w_gate_read, preferred_element_type=f32)
    arrived = []
    for part in range(2):
        reads = [None] * readers
        for k in list(range(1, readers)) + [0]:
            reads[k] = shifted_by(attend(queries[k], keys, values, held, part), "st", -k)
        out_mix = mix(mixed_in, gated, gate_mix, mix_weight, part)
        chunks = finish(reads, gate_read, out_mix, w_out_mix, w_out_read, near, part)
        base = near * (1 - part)
        arrived += [crossed_by(chunks[k], "tp", base + k) for k in range(near)]
    return functools.reduce(jnp.add, [piece.astype(f32) for piece in arrived]).astype(bf16)


def solution(mesh):
    placed = (
        P(("grp", "st"), None),
        P(),
        P(None, "tp"),
        P(None, "tp"),
        P("tp", None, None),
        P(None, "tp"),
        P(None, "tp"),
        P(None, "tp"),
        P(("grp", "st"), None, None),
        P(),
        P(None, "tp"),
        P(None, "tp"),
        P(("grp", "st"), None),
        P("tp", None),
        P("tp", None),
    )
    return jax.shard_map(
        local, mesh=mesh, in_specs=placed, out_specs=P(("grp", "st", "tp"), None), check_vma=False
    )
```

time: 79.8 us -> 96.6 us (1.21)
  the two profiles are of different devices: /device:TPU:9 before, /device:TPU:16 now
where the time goes in v2:
time: 96.6 us; the launch traced here: 96 us
  Pallas kernels  39.6 us (41%)
  waiting for transfers between devices  23 us (24%)
  matrix products  12.3 us (13%)
  starting transfers between devices  10.4 us (11%)
  other arithmetic  5.89 us (6%)
  local copies, waits for them, and re-layouts  4.68 us (5%)
    pallas_call x8, Pallas kernels, attend(): pl.pallas_call(functools.partial(attend_kernel, held=held, part=part), ou...  23.7 us
    ppermute x3, waiting for transfers between devices, crossed_by(): lax.ppermute(value, axis, [(i, i ^ mask) for i in range(lax.axis_size(axi...  23 us
    pallas_call x2, Pallas kernels, finish(): pl.pallas_call(functools.partial(finish_kernel, owners=len(parts), shares...  7.61 us
    ppermute x9, starting transfers between devices, shifted_by(): lax.ppermute(value, axis, [(i, (i + step) % count) for i in range(count)])  6.87 us
    unnamed x32, local copies, waits for them, and re-layouts  4.68 us
    pallas_call x2, Pallas kernels, mix(): pl.pallas_call(functools.partial(mix_kernel, part=part), out_shape=jax.Sh...  4.57 us
    pallas_call x1, Pallas kernels, make_queries(): pl.pallas_call(functools.partial(query_kernel, held=held), grid_spec=pltp...  3.81 us
    ppermute x3, starting transfers between devices, crossed_by(): lax.ppermute(value, axis, [(i, i ^ mask) for i in range(lax.axis_size(axi...  3.49 us
  transfers between devices with their start and end apart: 12, of which 3 were waited for; matrix products, arithmetic and copies ran while one was open for 17% of the time, Pallas kernels for 37%

profile of v2, /device:TPU:16, one launch (start us, length us, event | category | flops | bytes accessed | tf_op | source)
XLA Modules:
  0.0 96.0 jit_solution(13859473885143809631)
XLA Ops:
  0.0 3.8 %queries.1 = (bf16[256,2048]{1,0:T(8,128)(2,1)}, bf16[288,256]{1,0:T(8,128)(2,1)}) custom-call(s32[1]{0:T(128)} %bitcast.first_ref, s32[4,4]{1,0:T(4,128)} %ids_ref.1, bf16[256,2048]{1,0:T(8,128)(2,1)} %tokens_ref.1, f32[1,2048]{1,0:T(1,128)} %bitcast.17, bf16[2048,256]{1,0:T(8,128)(2,1)} %w_ref.1), custom_call_target="tpu_custom_call" | custom-call | flops 268435456 | bytes 3145728 | tf_op jit(solution)/shard_map/queries/pallas_call | solution.py:68
  3.8 1.0 %collective-permute-start.4 = (bf16[288,256]{1,0:T(8,128)(2,1)}, bf16[288,256]{1,0:T(8,128)(2,1)S(1)}, u32[]{:S(2)}, u32[]{:S(2)}) collective-permute-start(bf16[288,256]{1,0:T(8,128)(2,1)} %get-tuple-element.11.q_ref), channel_id=1, source_target_pairs={{0,12},{4,0},{8,4},{12,8},{1,13},{5,1},{9,5},{13,9},{2,14},{6,2},{... | collective-permute-start | bytes 442376 | tf_op jit(solution)/shard_map/ppermute | solution.py:261
  5.6 3.1 %fusion = f32[8,128]{1,0:T(8,128)S(1)} fusion(bf16[8,128,2048]{2,1,0:T(8,128)(2,1)} %param.23), kind=kLoop, calls=%fused_computation.2 | loop fusion | flops 6290432 | bytes 4198400 | tf_op jit(solution)/shard_map/reduce_sum | solution.py:29
  8.7 1.0 %fusion.2 = bf16[8,128,2048]{2,1,0:T(8,128)(2,1)S(1)} fusion(bf16[8,128,2048]{2,1,0:T(8,128)(2,1)S(1)} %copy-done.2, f32[2048]{0:T(1024)S(1)} %copy-done.13, f32[8,128]{1,0:T(8,128)S(1)} %add_rsqrt_fusion), kind=kLoop, calls=%fused_computation.4 | loop fusion | flops 8388608 | bytes 8400896 | tf_op jit(solution)/shard_map/convert_element_type | solution.py:30
  9.9 2.1 %convolution_convert_fusion.v_ref = bf16[1024,256]{1,0:T(8,128)(2,1)} fusion(bf16[1024,2048]{1,0:T(8,128)(2,1)S(1)} %bitcast.15, bf16[2048,256]{1,0:T(8,128)(2,1)S(1)} %copy-done.14), kind=kOutput, calls=%fused_computation.5 | convolution fusion | flops 1074003968 | bytes 5767168 | tf_op jit(solution)/shard_map/dot_general | solution.py:295
  12.0 2.0 %convolution_convert_fusion.1.k_ref = bf16[1024,256]{1,0:T(8,128)(2,1)} fusion(bf16[1024,2048]{1,0:T(8,128)(2,1)S(1)} %bitcast.16, bf16[2048,256]{1,0:T(8,128)(2,1)S(1)} %copy-done.15), kind=kOutput, calls=%fused_computation.6 | convolution fusion | flops 1074003968 | bytes 5767168 | tf_op jit(solution)/shard_map/dot_general | solution.py:294
  14.0 1.5 %fusion.6.gate_ref = f32[256,384]{1,0:T(8,128)} fusion(bf16[256,2048]{1,0:T(8,128)(2,1)S(1)} %copy-done.1, bf16[2048,384]{1,0:T(8,128)(2,1)S(1)} %copy-done), kind=kOutput, calls=%fused_computation.12 | convolution fusion | flops 402653184 | bytes 3014656 | tf_op jit(solution)/shard_map/dot_general | solution.py:298
  15.5 1.5 %fusion.5.gated_ref = f32[256,384]{1,0:T(8,128)} fusion(bf16[256,2048]{1,0:T(8,128)(2,1)S(1)} %copy-done.1, bf16[2048,384]{1,0:T(8,128)(2,1)S(1)} %copy-done.3), kind=kOutput, calls=%fused_computation.11 | convolution fusion | flops 402653184 | bytes 3014656 | tf_op jit(solution)/shard_map/dot_general | solution.py:296
  17.0 0.7 copy-done.6
  17.6 3.0 %attend.13 = bf16[144,256]{1,0:T(8,128)(2,1)} custom-call(bf16[288,256]{1,0:T(8,128)(2,1)} %copy-done.6, bf16[1024,256]{1,0:T(8,128)(2,1)} %convolution_convert_fusion.1.k_ref, bf16[1024,256]{1,0:T(8,128)(2,1)} %convolution_convert_fusion.v_ref), custom_call_target="tpu_custom_call" | custom-call | flops 134217728 | bytes 1343488 | tf_op jit(solution)/shard_map/attend/pallas_call | solution.py:139
  20.6 1.6 %collective-permute-start.8 = (bf16[144,256]{1,0:T(8,128)(2,1)}, bf16[144,256]{1,0:T(8,128)(2,1)S(1)}, u32[]{:S(2)}, u32[]{:S(2)}) collective-permute-start(bf16[144,256]{1,0:T(8,128)(2,1)} %attend.13), channel_id=1, source_target_pairs={{0,12},{4,0},{8,4},{12,8},{1,13},{5,1},{9,5},{13,9},{2,14},{6,2},{... | collective-permute-start | bytes 221192 | tf_op jit(solution)/shard_map/ppermute | solution.py:261
  22.2 2.9 %fusion.4.mixed_ref = f32[256,384]{1,0:T(8,128)} fusion(bf16[256,2048]{1,0:T(8,128)(2,1)S(1)} %copy-done.1, bf16[2048,384]{1,0:T(8,128)(2,1)} %param.18), kind=kOutput, calls=%fused_computation.10 | convolution fusion | flops 402653184 | bytes 3014656 | tf_op jit(solution)/shard_map/dot_general | solution.py:297
  25.0 3.0 %attend.9 = bf16[144,256]{1,0:T(8,128)(2,1)} custom-call(bf16[288,256]{1,0:T(8,128)(2,1)} %copy-done.6, bf16[1024,256]{1,0:T(8,128)(2,1)} %convolution_convert_fusion.1.k_ref, bf16[1024,256]{1,0:T(8,128)(2,1)} %convolution_convert_fusion.v_ref), custom_call_target="tpu_custom_call" | custom-call | flops 134217728 | bytes 1343488 | tf_op jit(solution)/shard_map/attend/pallas_call | solution.py:139
  28.7 3.0 %attend.10 = bf16[144,256]{1,0:T(8,128)(2,1)} custom-call(bf16[288,256]{1,0:T(8,128)(2,1)} %copy-done.5, bf16[1024,256]{1,0:T(8,128)(2,1)} %convolution_convert_fusion.1.k_ref, bf16[1024,256]{1,0:T(8,128)(2,1)} %convolution_convert_fusion.v_ref), custom_call_target="tpu_custom_call" | custom-call | flops 134217728 | bytes 1343488 | tf_op jit(solution)/shard_map/attend/pallas_call | solution.py:139
  31.6 1.4 %collective-permute-start.3 = (bf16[144,256]{1,0:T(8,128)(2,1)}, bf16[144,256]{1,0:T(8,128)(2,1)S(1)}, u32[]{:S(2)}, u32[]{:S(2)}) collective-permute-start(bf16[144,256]{1,0:T(8,128)(2,1)} %attend.10), channel_id=1, source_target_pairs={{0,8},{4,12},{8,0},{12,4},{1,9},{5,13},{9,1},{13,5},{2,10},{6,14},... | collective-permute-start | bytes 221192 | tf_op jit(solution)/shard_map/ppermute | solution.py:261
  33.0 2.9 %attend.14 = bf16[144,256]{1,0:T(8,128)(2,1)} custom-call(bf16[288,256]{1,0:T(8,128)(2,1)} %copy-done.5, bf16[1024,256]{1,0:T(8,128)(2,1)} %convolution_convert_fusion.1.k_ref, bf16[1024,256]{1,0:T(8,128)(2,1)} %convolution_convert_fusion.v_ref), custom_call_target="tpu_custom_call" | custom-call | flops 134217728 | bytes 1343488 | tf_op jit(solution)/shard_map/attend/pallas_call | solution.py:139
  36.6 0.7 copy-done.4
  37.3 3.0 %attend.11 = bf16[144,256]{1,0:T(8,128)(2,1)} custom-call(bf16[288,256]{1,0:T(8,128)(2,1)} %copy-done.4, bf16[1024,256]{1,0:T(8,128)(2,1)} %convolution_convert_fusion.1.k_ref, bf16[1024,256]{1,0:T(8,128)(2,1)} %convolution_convert_fusion.v_ref), custom_call_target="tpu_custom_call" | custom-call | flops 134217728 | bytes 1343488 | tf_op jit(solution)/shard_map/attend/pallas_call | solution.py:139
  40.2 3.0 %attend.15 = bf16[144,256]{1,0:T(8,128)(2,1)} custom-call(bf16[288,256]{1,0:T(8,128)(2,1)} %copy-done.4, bf16[1024,256]{1,0:T(8,128)(2,1)} %convolution_convert_fusion.1.k_ref, bf16[1024,256]{1,0:T(8,128)(2,1)} %convolution_convert_fusion.v_ref), custom_call_target="tpu_custom_call" | custom-call | flops 134217728 | bytes 1343488 | tf_op jit(solution)/shard_map/attend/pallas_call | solution.py:139
  43.2 1.5 %collective-permute-start.10 = (bf16[144,256]{1,0:T(8,128)(2,1)}, bf16[144,256]{1,0:T(8,128)(2,1)S(1)}, u32[]{:S(2)}, u32[]{:S(2)}) collective-permute-start(bf16[144,256]{1,0:T(8,128)(2,1)} %attend.15), channel_id=1, source_target_pairs={{0,4},{4,8},{8,12},{12,0},{1,5},{5,9},{9,13},{13,1},{2,6},{6,10},{... | collective-permute-start | bytes 221192 | tf_op jit(solution)/shard_map/ppermute | solution.py:261
  44.7 2.4 %fusion.3.refs_4_ = f32[256,256]{1,0:T(8,128)} fusion(bf16[256,2048]{1,0:T(8,128)(2,1)S(1)} %copy-done.1, bf16[2048,256]{1,0:T(8,128)(2,1)} %param.22), kind=kOutput, calls=%fused_computation.9 | convolution fusion | flops 268435456 | bytes 2359296 | tf_op jit(solution)/shard_map/dot_general | solution.py:299
  47.1 2.3 %mix.3.refs_5_ = bf16[128,384]{1,0:T(8,128)(2,1)} custom-call(f32[256,384]{1,0:T(8,128)} %fusion.4.mixed_ref, f32[256,384]{1,0:T(8,128)} %fusion.5.gated_ref, f32[256,384]{1,0:T(8,128)} %fusion.6.gate_ref, bf16[2,128,128]{2,1,0:T(8,128)(2,1)} %mixw_ref.3), custom_call_target="tpu_custom_call" | custom-call | flops 26148864 | bytes 688128 | tf_op jit(solution)/shard_map/mix/pallas_call | solution.py:188
  49.3 2.3 %mix.2.refs_5_ = bf16[128,384]{1,0:T(8,128)(2,1)} custom-call(f32[256,384]{1,0:T(8,128)} %fusion.4.mixed_ref, f32[256,384]{1,0:T(8,128)} %fusion.5.gated_ref, f32[256,384]{1,0:T(8,128)} %fusion.6.gate_ref, bf16[2,128,128]{2,1,0:T(8,128)(2,1)} %mixw_ref.3), custom_call_target="tpu_custom_call" | custom-call | flops 26148864 | bytes 688128 | tf_op jit(solution)/shard_map/mix/pallas_call | solution.py:188
  51.6 3.0 %attend.12.refs_0_ = bf16[144,256]{1,0:T(8,128)(2,1)} custom-call(bf16[288,256]{1,0:T(8,128)(2,1)} %get-tuple-element.11.q_ref, bf16[1024,256]{1,0:T(8,128)(2,1)} %convolution_convert_fusion.1.k_ref, bf16[1024,256]{1,0:T(8,128)(2,1)} %convolution_convert_fusion.v_ref), custom_call_target="tpu_custom_call" | custom-call | flops 134217728 | bytes 1343488 | tf_op jit(solution)/shard_map/attend/pallas_call | solution.py:139
  54.6 3.0 %attend.8.refs_0_ = bf16[144,256]{1,0:T(8,128)(2,1)} custom-call(bf16[288,256]{1,0:T(8,128)(2,1)} %get-tuple-element.11.q_ref, bf16[1024,256]{1,0:T(8,128)(2,1)} %convolution_convert_fusion.1.k_ref, bf16[1024,256]{1,0:T(8,128)(2,1)} %convolution_convert_fusion.v_ref), custom_call_target="tpu_custom_call" | custom-call | flops 134217728 | bytes 1343488 | tf_op jit(solution)/shard_map/attend/pallas_call | solution.py:139
  58.8 3.8 %finish.3 = (bf16[64,2048]{1,0:T(8,128)(2,1)}, bf16[64,2048]{1,0:T(8,128)(2,1)}) custom-call(bf16[144,256]{1,0:T(8,128)(2,1)} %attend.12.refs_0_, bf16[144,256]{1,0:T(8,128)(2,1)} %copy-done.9, bf16[144,256]{1,0:T(8,128)(2,1)} %copy-done.11, bf16[144,256]{1,0:T(8,128)(2,1)} %copy-done.12, f32[256,256]{1,0:T(8,128)} %fusion.3.refs_4_, ...), custom_call_target="tpu_custom_call" | custom-call | flops 335544320 | bytes 3145728 | tf_op jit(solution)/shard_map/finish/pallas_call | solution.py:242
  62.6 1.6 %collective-permute-start.11 = (bf16[64,2048]{1,0:T(8,128)(2,1)}, bf16[64,2048]{1,0:T(8,128)(2,1)S(1)}, u32[]{:S(2)}, u32[]{:S(2)}) collective-permute-start(bf16[64,2048]{1,0:T(8,128)(2,1)} %get-tuple-element.16), channel_id=1, source_target_pairs={{0,1},{1,0},{2,3},{3,2},{4,5},{5,4},{6,7},{7,6},{8,9},{9,8},{10,11... | collective-permute-start | bytes 786440 | tf_op jit(solution)/shard_map/ppermute | solution.py:267
  65.5 3.8 %finish.2 = (bf16[64,2048]{1,0:T(8,128)(2,1)}, bf16[64,2048]{1,0:T(8,128)(2,1)}) custom-call(bf16[144,256]{1,0:T(8,128)(2,1)} %attend.8.refs_0_, bf16[144,256]{1,0:T(8,128)(2,1)} %copy-done.7, bf16[144,256]{1,0:T(8,128)(2,1)} %copy-done.8, bf16[144,256]{1,0:T(8,128)(2,1)} %copy-done.10, f32[256,256]{1,0:T(8,128)} %fusion.3.refs_4_, ...), custom_call_target="tpu_custom_call" | custom-call | flops 335544320 | bytes 3145728 | tf_op jit(solution)/shard_map/finish/pallas_call | solution.py:242
  69.6 1.6 %collective-permute-start.7 = (bf16[64,2048]{1,0:T(8,128)(2,1)}, bf16[64,2048]{1,0:T(8,128)(2,1)S(1)}, u32[]{:S(2)}, u32[]{:S(2)}) collective-permute-start(bf16[64,2048]{1,0:T(8,128)(2,1)} %get-tuple-element.14), channel_id=1, source_target_pairs={{0,3},{1,2},{2,1},{3,0},{4,7},{5,6},{6,5},{7,4},{8,11},{9,10},{10,... | collective-permute-start | bytes 786440 | tf_op jit(solution)/shard_map/ppermute | solution.py:267
  71.5 15.6 %collective-permute-done.6 = bf16[64,2048]{1,0:T(8,128)(2,1)S(1)} collective-permute-done((bf16[64,2048]{1,0:T(8,128)(2,1)}, bf16[64,2048]{1,0:T(8,128)(2,1)S(1)}, u32[]{:S(2)}, u32[]{:S(2)}) %collective-permute-start.6) | collective-permute-done | bytes 262176 | tf_op jit(solution)/shard_map/ppermute | solution.py:267
  87.1 7.1 %collective-permute-done.7 = bf16[64,2048]{1,0:T(8,128)(2,1)S(1)} collective-permute-done((bf16[64,2048]{1,0:T(8,128)(2,1)}, bf16[64,2048]{1,0:T(8,128)(2,1)S(1)}, u32[]{:S(2)}, u32[]{:S(2)}) %collective-permute-start.7) | collective-permute-done | bytes 262176 | tf_op jit(solution)/shard_map/ppermute | solution.py:267
  94.2 1.8 %add_convert_fusion = bf16[64,2048]{1,0:T(8,128)(2,1)} fusion(bf16[64,2048]{1,0:T(8,128)(2,1)S(1)} %collective-permute-done.11, bf16[64,2048]{1,0:T(8,128)(2,1)} %get-tuple-element.15, bf16[64,2048]{1,0:T(8,128)(2,1)S(1)} %collective-permute-done.7, bf16[64,2048]{1,0:T(8,128)(2,1)S(1)} %collective-permute-done.6), kind=kLoop, calls=%fused_computation.7 | loop fusion | flops 1048576 | bytes 1310720 | tf_op jit(solution)/shard_map/convert_element_type | solution.py:309
  (47 shorter events, 5.5 us)
Async XLA Ops:
  0.0 14.0 %copy-start = (bf16[2048,384]{1,0:T(8,128)(2,1)S(1)}, bf16[2048,384]{1,0:T(8,128)(2,1)}, u32[]{:S(2)}) copy-start(bf16[2048,384]{1,0:T(8,128)(2,1)} %param.21) | copy-start | bytes 4718596
  0.0 8.7 %copy-start.13 = (f32[2048]{0:T(1024)S(1)}, f32[2048]{0:T(1024)}, u32[]{:S(2)}) copy-start(f32[2048]{0:T(1024)} %param.24) | copy-start | bytes 24580
  3.8 4.9 %copy-start.2 = (bf16[8,128,2048]{2,1,0:T(8,128)(2,1)S(1)}, bf16[8,128,2048]{2,1,0:T(8,128)(2,1)}, u32[]{:S(2)}) copy-start(bf16[8,128,2048]{2,1,0:T(8,128)(2,1)} %param.23) | copy-start | bytes 12582916
  3.8 32.8 %collective-permute-start.4 = (bf16[288,256]{1,0:T(8,128)(2,1)}, bf16[288,256]{1,0:T(8,128)(2,1)S(1)}, u32[]{:S(2)}, u32[]{:S(2)}) collective-permute-start(bf16[288,256]{1,0:T(8,128)(2,1)} %get-tuple-element.11.q_ref), channel_id=1, source_target_pairs={{0,12},{4,0},{8,4},{12,8},{1,13},{5,1},{9,5},{13,9},{2,14},{6,2},{... | collective-permute-start | bytes 442376 | tf_op jit(solution)/shard_map/ppermute | solution.py:261
  4.8 23.2 %collective-permute-start.2 = (bf16[288,256]{1,0:T(8,128)(2,1)}, bf16[288,256]{1,0:T(8,128)(2,1)S(1)}, u32[]{:S(2)}, u32[]{:S(2)}) collective-permute-start(bf16[288,256]{1,0:T(8,128)(2,1)} %get-tuple-element.11.q_ref), channel_id=1, source_target_pairs={{0,8},{4,12},{8,0},{12,4},{1,9},{5,13},{9,1},{13,5},{2,10},{6,14},... | collective-permute-start | bytes 442376 | tf_op jit(solution)/shard_map/ppermute | solution.py:261
  5.4 11.6 %collective-permute-start = (bf16[288,256]{1,0:T(8,128)(2,1)}, bf16[288,256]{1,0:T(8,128)(2,1)S(1)}, u32[]{:S(2)}, u32[]{:S(2)}) collective-permute-start(bf16[288,256]{1,0:T(8,128)(2,1)} %get-tuple-element.11.q_ref), channel_id=1, source_target_pairs={{0,4},{4,8},{8,12},{12,0},{1,5},{5,9},{9,13},{13,1},{2,6},{6,10},{... | collective-permute-start | bytes 442376 | tf_op jit(solution)/shard_map/ppermute | solution.py:261
  8.7 1.2 %copy-start.14 = (bf16[2048,256]{1,0:T(8,128)(2,1)S(1)}, bf16[2048,256]{1,0:T(8,128)(2,1)}, u32[]{:S(2)}) copy-start(bf16[2048,256]{1,0:T(8,128)(2,1)} %param.26) | copy-start | bytes 3145732
  9.7 2.2 %copy-start.15 = (bf16[2048,256]{1,0:T(8,128)(2,1)S(1)}, bf16[2048,256]{1,0:T(8,128)(2,1)}, u32[]{:S(2)}) copy-start(bf16[2048,256]{1,0:T(8,128)(2,1)} %param.25) | copy-start | bytes 3145732
  12.0 2.1 %copy-start.1 = (bf16[256,2048]{1,0:T(8,128)(2,1)S(1)}, bf16[256,2048]{1,0:T(8,128)(2,1)}, u32[]{:S(2)}) copy-start(bf16[256,2048]{1,0:T(8,128)(2,1)} %get-tuple-element.12) | copy-start | bytes 3145732
  12.0 3.5 %copy-start.3 = (bf16[2048,384]{1,0:T(8,128)(2,1)S(1)}, bf16[2048,384]{1,0:T(8,128)(2,1)}, u32[]{:S(2)}) copy-start(bf16[2048,384]{1,0:T(8,128)(2,1)} %param.17) | copy-start | bytes 4718596
  17.0 0.7 copy-start.6
  20.6 22.6 %collective-permute-start.8 = (bf16[144,256]{1,0:T(8,128)(2,1)}, bf16[144,256]{1,0:T(8,128)(2,1)S(1)}, u32[]{:S(2)}, u32[]{:S(2)}) collective-permute-start(bf16[144,256]{1,0:T(8,128)(2,1)} %attend.13), channel_id=1, source_target_pairs={{0,12},{4,0},{8,4},{12,8},{1,13},{5,1},{9,5},{13,9},{2,14},{6,2},{... | collective-permute-start | bytes 221192 | tf_op jit(solution)/shard_map/ppermute | solution.py:261
  28.0 36.2 %collective-permute-start.1 = (bf16[144,256]{1,0:T(8,128)(2,1)}, bf16[144,256]{1,0:T(8,128)(2,1)S(1)}, u32[]{:S(2)}, u32[]{:S(2)}) collective-permute-start(bf16[144,256]{1,0:T(8,128)(2,1)} %attend.9), channel_id=1, source_target_pairs={{0,12},{4,0},{8,4},{12,8},{1,13},{5,1},{9,5},{13,9},{2,14},{6,2},{... | collective-permute-start | bytes 221192 | tf_op jit(solution)/shard_map/ppermute | solution.py:261
  28.0 0.7 copy-start.5
  31.6 32.6 %collective-permute-start.3 = (bf16[144,256]{1,0:T(8,128)(2,1)}, bf16[144,256]{1,0:T(8,128)(2,1)S(1)}, u32[]{:S(2)}, u32[]{:S(2)}) collective-permute-start(bf16[144,256]{1,0:T(8,128)(2,1)} %attend.10), channel_id=1, source_target_pairs={{0,8},{4,12},{8,0},{12,4},{1,9},{5,13},{9,1},{13,5},{2,10},{6,14},... | collective-permute-start | bytes 221192 | tf_op jit(solution)/shard_map/ppermute | solution.py:261
  36.0 21.6 %collective-permute-start.9 = (bf16[144,256]{1,0:T(8,128)(2,1)}, bf16[144,256]{1,0:T(8,128)(2,1)S(1)}, u32[]{:S(2)}, u32[]{:S(2)}) collective-permute-start(bf16[144,256]{1,0:T(8,128)(2,1)} %attend.14), channel_id=1, source_target_pairs={{0,8},{4,12},{8,0},{12,4},{1,9},{5,13},{9,1},{13,5},{2,10},{6,14},... | collective-permute-start | bytes 221192 | tf_op jit(solution)/shard_map/ppermute | solution.py:261
  36.6 0.7 copy-start.4
  40.2 24.0 %collective-permute-start.5 = (bf16[144,256]{1,0:T(8,128)(2,1)}, bf16[144,256]{1,0:T(8,128)(2,1)S(1)}, u32[]{:S(2)}, u32[]{:S(2)}) collective-permute-start(bf16[144,256]{1,0:T(8,128)(2,1)} %attend.11), channel_id=1, source_target_pairs={{0,4},{4,8},{8,12},{12,0},{1,5},{5,9},{9,13},{13,1},{2,6},{6,10},{... | collective-permute-start | bytes 221192 | tf_op jit(solution)/shard_map/ppermute | solution.py:261
  43.2 14.4 %copy-start.9 = (bf16[144,256]{1,0:T(8,128)(2,1)}, bf16[144,256]{1,0:T(8,128)(2,1)S(1)}, u32[]{:S(2)}) copy-start(bf16[144,256]{1,0:T(8,128)(2,1)S(1)} %collective-permute-done.8.refs_1_) | copy-start | bytes 221188
  43.2 14.4 %collective-permute-start.10 = (bf16[144,256]{1,0:T(8,128)(2,1)}, bf16[144,256]{1,0:T(8,128)(2,1)S(1)}, u32[]{:S(2)}, u32[]{:S(2)}) collective-permute-start(bf16[144,256]{1,0:T(8,128)(2,1)} %attend.15), channel_id=1, source_target_pairs={{0,4},{4,8},{8,12},{12,0},{1,5},{5,9},{9,13},{13,1},{2,6},{6,10},{... | collective-permute-start | bytes 221192 | tf_op jit(solution)/shard_map/ppermute | solution.py:261
  57.6 0.6 copy-start.11
  58.2 0.6 copy-start.12
  62.6 8.9 %collective-permute-start.11 = (bf16[64,2048]{1,0:T(8,128)(2,1)}, bf16[64,2048]{1,0:T(8,128)(2,1)S(1)}, u32[]{:S(2)}, u32[]{:S(2)}) collective-permute-start(bf16[64,2048]{1,0:T(8,128)(2,1)} %get-tuple-element.16), channel_id=1, source_target_pairs={{0,1},{1,0},{2,3},{3,2},{4,5},{5,4},{6,7},{7,6},{8,9},{9,8},{10,11... | collective-permute-start | bytes 786440 | tf_op jit(solution)/shard_map/ppermute | solution.py:267
  64.2 0.6 copy-start.7
  64.2 0.7 copy-start.8
  64.8 0.6 copy-start.10
  69.3 17.8 %collective-permute-start.6 = (bf16[64,2048]{1,0:T(8,128)(2,1)}, bf16[64,2048]{1,0:T(8,128)(2,1)S(1)}, u32[]{:S(2)}, u32[]{:S(2)}) collective-permute-start(bf16[64,2048]{1,0:T(8,128)(2,1)} %get-tuple-element.13), channel_id=1, source_target_pairs={{0,2},{1,3},{2,0},{3,1},{4,6},{5,7},{6,4},{7,5},{8,10},{9,11},{10,... | collective-permute-start | bytes 786440 | tf_op jit(solution)/shard_map/ppermute | solution.py:267
  69.6 24.6 %collective-permute-start.7 = (bf16[64,2048]{1,0:T(8,128)(2,1)}, bf16[64,2048]{1,0:T(8,128)(2,1)S(1)}, u32[]{:S(2)}, u32[]{:S(2)}) collective-permute-start(bf16[64,2048]{1,0:T(8,128)(2,1)} %get-tuple-element.14), channel_id=1, source_target_pairs={{0,3},{1,2},{2,1},{3,0},{4,7},{5,6},{6,5},{7,4},{8,11},{9,10},{10,... | collective-permute-start | bytes 786440 | tf_op jit(solution)/shard_map/ppermute | solution.py:267

commit v3 on v2

--- a/solution.py
+++ b/solution.py
@@ -93,69 +93,107 @@
     )(first, ids, tokens, gain.reshape(1, -1), w_query)
 
 
-def attend_kernel(q_ref, k_ref, v_ref, out_ref, *, held, part):
-    rows = out_ref.shape[0] - EXTRA
-    width = out_ref.shape[1]
+def store_kernel(rows_ref, gain_ref, wk_ref, wv_ref, k_ref, v_ref):
+    rows = row_norm(rows_ref[...], gain_ref[...])
+    k_ref[...] = jnp.dot(rows, wk_ref[...], preferred_element_type=f32).astype(bf16)
+    v_ref[...] = jnp.dot(rows, wv_ref[...], preferred_element_type=f32).astype(bf16)
+
+
+def project_store(store, gain, w_key, w_value):
+    model = store.shape[-1]
+    flat = store.reshape(-1, model)
+    width = w_key.shape[1]
+    step = 2 * PROWS
+    whole = pl.BlockSpec((model, width), lambda i: (0, 0))
+    tile = pl.BlockSpec((step, width), lambda i: (i, 0))
+    out = jax.ShapeDtypeStruct((flat.shape[0], width), bf16)
+    return pl.pallas_call(
+        store_kernel,
+        grid=(flat.shape[0] // step,),
+        in_specs=[
+            pl.BlockSpec((step, model), lambda i: (i, 0)),
+            pl.BlockSpec((1, model), lambda i: (0, 0)),
+            whole,
+            whole,
+        ],
+        out_specs=[tile, tile],
+        out_shape=[out, out],
+        cost_estimate=pl.CostEstimate(
+            flops=4 * flat.size * width,
+            transcendentals=flat.shape[0],
+            bytes_accessed=2 * (flat.size + 2 * w_key.size + 2 * flat.shape[0] * width),
+        ),
+        name="project_store",
+    )(flat, gain.reshape(1, -1), w_key, w_value)
+
+
+def attend_kernel(*refs, readers, held, part):
+    queries = refs[:readers]
+    k_ref, v_ref = refs[readers : readers + 2]
+    outs = refs[readers + 2 :]
+    rows = outs[0].shape[0] - EXTRA
+    width = outs[0].shape[1]
     start = part * (rows + EXTRA)
     here = lax.axis_index("st").astype(f32)
-    table = q_ref[start + rows : start + rows + EXTRA, :rows].astype(f32)
     passage = lax.broadcasted_iota(jnp.int32, (held, rows), 0).astype(f32)
-    count = jnp.zeros((held, rows), f32)
-    for j in range(NPB):
-        mine = table[2 * j : 2 * j + 1] == here
-        hit = (passage == table[2 * j + 1 : 2 * j + 2]) & mine
-        count = count + jnp.where(hit, 1.0, 0.0)
-    bias = jnp.where(count > 0.0, jnp.log2(jnp.maximum(count, 1.0)), FAR)
     which = lax.broadcasted_iota(jnp.int32, (EXTRA, rows), 0)
-    for h in range(width // HD):
-        cols = slice(h * HD, (h + 1) * HD)
-        scores = lax.dot_general(
-            k_ref[:, cols],
-            q_ref[start : start + rows, cols],
-            (((1,), (1,)), ((), ())),
-            preferred_element_type=f32,
-        ) * (HD ** (-0.5) * LOG2E)
-        shifted = scores.reshape(held, PROWS, rows) + bias[:, None, :]
-        top = jnp.max(jnp.max(shifted, axis=0), axis=0, keepdims=True)
-        weights = jnp.exp2(shifted - top[None])
-        total = jnp.sum(jnp.sum(weights, axis=0), axis=0, keepdims=True)
-        read = lax.dot_general(
-            weights.astype(bf16).reshape(held * PROWS, rows),
-            v_ref[:, cols],
-            (((0,), (0,)), ((), ())),
-            preferred_element_type=f32,
-        )
-        out_ref[:rows, cols] = read.astype(bf16)
-        stats = jnp.zeros((EXTRA, rows), f32)
-        for i, piece in enumerate(pieces_of(top) + pieces_of(total)):
-            stats = jnp.where(which == i, piece, stats)
-        out_ref[rows:, h * HD : h * HD + rows] = stats.astype(bf16)
-
-
-def attend(query, keys, values, held, part):
-    rows = query.shape[0] // 2 - EXTRA
-    width = query.shape[1]
+    for q_ref, out_ref in zip(queries, outs):
+        table = q_ref[start + rows : start + rows + EXTRA, :rows].astype(f32)
+        count = jnp.zeros((held, rows), f32)
+        for j in range(NPB):
+            mine = table[2 * j : 2 * j + 1] == here
+            hit = (passage == table[2 * j + 1 : 2 * j + 2]) & mine
+            count = count + jnp.where(hit, 1.0, 0.0)
+        bias = jnp.where(count > 0.0, jnp.log2(jnp.maximum(count, 1.0)), FAR)
+        for h in range(width // HD):
+            cols = slice(h * HD, (h + 1) * HD)
+            scores = lax.dot_general(
+                k_ref[:, cols],
+                q_ref[start : start + rows, cols],
+                (((1,), (1,)), ((), ())),
+                preferred_element_type=f32,
+            ) * (HD ** (-0.5) * LOG2E)
+            shifted = scores.reshape(held, PROWS, rows) + bias[:, None, :]
+            top = jnp.max(jnp.max(shifted, axis=0), axis=0, keepdims=True)
+            weights = jnp.exp2(shifted - top[None])
+            total = jnp.sum(jnp.sum(weights, axis=0), axis=0, keepdims=True)
+            read = lax.dot_general(
+                weights.astype(bf16).reshape(held * PROWS, rows),
+                v_ref[:, cols],
+                (((0,), (0,)), ((), ())),
+                preferred_element_type=f32,
+            )
+            out_ref[:rows, cols] = read.astype(bf16)
+            stats = jnp.zeros((EXTRA, rows), f32)
+            for i, piece in enumerate(pieces_of(top) + pieces_of(total)):
+                stats = jnp.where(which == i, piece, stats)
+            out_ref[rows:, h * HD : h * HD + rows] = stats.astype(bf16)
+
+
+def attend(queries, keys, values, held, part):
+    readers = len(queries)
+    rows = queries[0].shape[0] // 2 - EXTRA
+    width = queries[0].shape[1]
     assert rows == HD
     return pl.pallas_call(
-        functools.partial(attend_kernel, held=held, part=part),
-        out_shape=jax.ShapeDtypeStruct((rows + EXTRA, width), bf16),
-        in_specs=[pl.BlockSpec(memory_space=pltpu.VMEM)] * 3,
-        out_specs=pl.BlockSpec(memory_space=pltpu.VMEM),
-        cost_estimate=pl.CostEstimate(
-            flops=4 * rows * keys.shape[0] * width,
-            transcendentals=rows * keys.shape[0] * (width // HD),
-            bytes_accessed=2 * (2 * keys.size + 2 * query.size),
+        functools.partial(attend_kernel, readers=readers, held=held, part=part),
+        out_shape=[jax.ShapeDtypeStruct((rows + EXTRA, width), bf16)] * readers,
+        in_specs=[pl.BlockSpec(memory_space=pltpu.VMEM)] * (readers + 2),
+        out_specs=[pl.BlockSpec(memory_space=pltpu.VMEM)] * readers,
+        cost_estimate=pl.CostEstimate(
+            flops=4 * readers * rows * keys.shape[0] * width,
+            transcendentals=readers * rows * keys.shape[0] * (width // HD),
+            bytes_accessed=2 * (2 * keys.size + 2 * readers * queries[0].size),
         ),
         name="attend",
-    )(query, keys, values)
-
-
-def mix_kernel(mixed_ref, gated_ref, gate_ref, mixw_ref, out_ref, *, part):
+    )(*queries, keys, values)
+
+
+def mix_kernel(mixed_ref, gated_ref, gate_ref, mixw_ref, out_ref):
     rows, width = out_ref.shape
     groups = mixw_ref.shape[0]
     group_width = width // groups
-    start = part * rows
-    mixed = mixed_ref[start : start + rows, :]
+    mixed = mixed_ref[...]
     lane = lax.broadcasted_iota(jnp.int32, (1, width), 1) // group_width
     inside = [lane == g for g in range(groups)]
 
@@ -174,26 +212,25 @@
     masked = [jnp.where(below, mixw_ref[g].astype(f32), 0.0).astype(bf16) for g in range(groups)]
     for n in range(rows // SPAN):
         block = slice(n * SPAN, (n + 1) * SPAN)
-        source = slice(start + n * SPAN, start + (n + 1) * SPAN)
         spatial = jnp.zeros((SPAN, width), f32)
         for g in range(groups):
             spatial = jnp.where(
                 inside[g], jnp.dot(masked[g], normal[block], preferred_element_type=f32), spatial
             )
-        out_ref[block, :] = (gated_ref[source, :] * spatial * silu(gate_ref[source, :])).astype(bf16)
-
-
-def mix(mixed_in, gated, gate_mix, mix_weight, part):
+        out_ref[block, :] = (gated_ref[block, :] * spatial * silu(gate_ref[block, :])).astype(bf16)
+
+
+def mix(mixed_in, gated, gate_mix, mix_weight):
     rows, width = mixed_in.shape
     return pl.pallas_call(
-        functools.partial(mix_kernel, part=part),
-        out_shape=jax.ShapeDtypeStruct((rows // 2, width), bf16),
+        mix_kernel,
+        out_shape=jax.ShapeDtypeStruct((rows, width), bf16),
         in_specs=[pl.BlockSpec(memory_space=pltpu.VMEM)] * 4,
         out_specs=pl.BlockSpec(memory_space=pltpu.VMEM),
         cost_estimate=pl.CostEstimate(
-            flops=mixed_in.size * SPAN * mix_weight.shape[0] + 10 * mixed_in.size,
-            transcendentals=mixed_in.size // 2,
-            bytes_accessed=7 * mixed_in.size,
+            flops=2 * mixed_in.size * SPAN * mix_weight.shape[0] + 20 * mixed_in.size,
+            transcendentals=mixed_in.size,
+            bytes_accessed=14 * mixed_in.size,
         ),
         name="mix",
     )(mixed_in, gated, gate_mix, mix_weight)
@@ -204,7 +241,7 @@
     gate_ref, mix_ref, w_mix_ref, w_read_ref = refs[owners : owners + 4]
     outs = refs[owners + 4 : owners + 4 + shares]
     whole_ref = refs[owners + 4 + shares]
-    rows = mix_ref.shape[0]
+    rows = mix_ref.shape[0] // 2
     width = gate_ref.shape[1]
     out_read = []
     for h in range(width // HD):
@@ -224,7 +261,8 @@
             read = read + columns[:, i : i + 1] * p[:rows, cols].astype(f32)
         out_read.append((read * silu(gate_ref[part * rows : (part + 1) * rows, cols])).astype(bf16))
     out_read = out_read[0] if len(out_read) == 1 else jnp.concatenate(out_read, axis=1)
-    partial = jnp.dot(mix_ref[...], w_mix_ref[...], preferred_element_type=f32) + jnp.dot(
+    partial = jnp.dot(
+        mix_ref[part * rows : (part + 1) * rows, :], w_mix_ref[...], preferred_element_type=f32) + jnp.dot(
         out_read, w_read_ref[...], preferred_element_type=f32
     )
     whole_ref[...] = partial.astype(bf16)
@@ -236,7 +274,7 @@
 
 
 def finish(parts, gate_read, out_mix, w_out_mix, w_out_read, shares, part):
-    rows = out_mix.shape[0]
+    rows = out_mix.shape[0] // 2
     model = w_out_mix.shape[1]
     share = jax.ShapeDtypeStruct((rows // shares, model), bf16)
     return pl.pallas_call(
@@ -290,21 +328,23 @@
     first = (1 - lax.axis_index("tp") // near).astype(jnp.int32).reshape(1)
     normed, query = make_queries(first, passage_ids, tokens, pre_gain, w_query, held)
     queries = [shifted_by(query, "st", k) for k in range(readers)]
-    held_rows = lax.optimization_barrier(row_norm(store, mem_gain).reshape(-1, store.shape[-1]))
-    keys = jnp.dot(held_rows, w_key, preferred_element_type=f32).astype(bf16)
-    values = jnp.dot(held_rows, w_value, preferred_element_type=f32).astype(bf16)
-    gated = jnp.dot(normed, w_gated, preferred_element_type=f32)
-    mixed_in = jnp.dot(normed, w_mixed, preferred_element_type=f32)
+    keys, values = project_store(store, mem_gain, w_key, w_value)
     gate_mix = jnp.dot(normed, w_gate_mix, preferred_element_type=f32)
-    gate_read = jnp.dot(normed, w_gate_read, preferred_element_type=f32)
     arrived = []
     for part in range(2):
-        reads = [None] * readers
-        for k in list(range(1, readers)) + [0]:
-            reads[k] = shifted_by(attend(queries[k], keys, values, held, part), "st", -k)
-        out_mix = mix(mixed_in, gated, gate_mix, mix_weight, part)
+        reads = attend(queries, keys, values, held, part)
+        if part == 0:
+            reads, normed = lax.optimization_barrier((reads, normed))
+        reads = [shifted_by(reads[k], "st", -k) for k in range(readers)]
+        if part == 0:
+            gated = jnp.dot(normed, w_gated, preferred_element_type=f32)
+            mixed_in = jnp.dot(normed, w_mixed, preferred_element_type=f32)
+            gate_read = jnp.dot(normed, w_gate_read, preferred_element_type=f32)
+            out_mix = mix(mixed_in, gated, gate_mix, mix_weight)
         chunks = finish(reads, gate_read, out_mix, w_out_mix, w_out_read, near, part)
         base = near * (1 - part)
+        if part == 0:
+            chunks, queries = lax.optimization_barrier((chunks, queries))
         arrived += [crossed_by(chunks[k], "tp", base + k) for k in range(near)]
     return functools.reduce(jnp.add, [piece.astype(f32) for piece in arrived]).astype(bf16)
 

time: 96.6 us -> 71.5 us (0.74)
  the two profiles are of different devices: /device:TPU:16 before, /device:TPU:0 now
where the time goes in v3:
time: 71.5 us; the launch traced here: 71.1 us
  Pallas kernels  29.6 us (41%)
  waiting for transfers between devices  15.5 us (22%)
  starting transfers between devices  13.5 us (19%)
  matrix products  8.28 us (12%)
  local copies, waits for them, and re-layouts  2.4 us (3%)
  other arithmetic  1.79 us (3%)
    ppermute x3, waiting for transfers between devices, crossed_by(): lax.ppermute(value, axis, [(i, i ^ mask) for i in range(lax.axis_size(axi...  14.3 us
    pallas_call x2, Pallas kernels, attend(): pl.pallas_call(functools.partial(attend_kernel, readers=readers, held=hel...  8.89 us
    ppermute x9, starting transfers between devices, shifted_by(): lax.ppermute(value, axis, [(i, (i + step) % count) for i in range(count)])  8.14 us
    pallas_call x2, Pallas kernels, finish(): pl.pallas_call(functools.partial(finish_kernel, owners=len(parts), shares...  7.65 us
    pallas_call x1, Pallas kernels, project_store(): pl.pallas_call(store_kernel, grid=(flat.shape[0] // step,), in_specs=[pl....  6.79 us
    ppermute x3, starting transfers between devices, crossed_by(): lax.ppermute(value, axis, [(i, i ^ mask) for i in range(lax.axis_size(axi...  5.31 us
    pallas_call x1, Pallas kernels, make_queries(): pl.pallas_call(functools.partial(query_kernel, held=held), grid_spec=pltp...  3.8 us
    dot_general x1, matrix products, local(): mixed_in = jnp.dot(normed, w_mixed, preferred_element_type=f32)  2.98 us
  transfers between devices with their start and end apart: 12, of which 4 were waited for; matrix products, arithmetic and copies ran while one was open for 5% of the time, Pallas kernels for 18%

profile of v3, /device:TPU:0, one launch (start us, length us, event | category | flops | bytes accessed | tf_op | source)
XLA Modules:
  0.0 71.1 jit_solution(13760096932623677386)
XLA Ops:
  0.0 3.8 %queries.1 = (bf16[256,2048]{1,0:T(8,128)(2,1)}, bf16[288,256]{1,0:T(8,128)(2,1)}) custom-call(s32[1]{0:T(128)} %bitcast.first_ref, s32[4,4]{1,0:T(4,128)} %ids_ref.1, bf16[256,2048]{1,0:T(8,128)(2,1)} %tokens_ref.1, f32[1,2048]{1,0:T(1,128)} %bitcast.12, bf16[2048,256]{1,0:T(8,128)(2,1)} %w_ref.1), custom_call_target="tpu_custom_call" | custom-call | flops 268435456 | bytes 3145728 | tf_op jit(solution)/shard_map/queries/pallas_call | solution.py:68
  3.8 0.5 collective-permute-start
  4.3 2.6 %collective-permute-start.1 = (bf16[288,256]{1,0:T(8,128)(2,1)}, bf16[288,256]{1,0:T(8,128)(2,1)S(1)}, u32[]{:S(2)}, u32[]{:S(2)}) collective-permute-start(bf16[288,256]{1,0:T(8,128)(2,1)} %get-tuple-element.49.refs_0_), channel_id=1, source_target_pairs={{0,8},{4,12},{8,0},{12,4},{1,9},{5,13},{9,1},{13,5},{2,10},{6,14},... | collective-permute-start | bytes 442376 | tf_op jit(solution)/shard_map/ppermute | solution.py:299
  6.8 1.4 %collective-permute-start.2 = (bf16[288,256]{1,0:T(8,128)(2,1)}, bf16[288,256]{1,0:T(8,128)(2,1)S(1)}, u32[]{:S(2)}, u32[]{:S(2)}) collective-permute-start(bf16[288,256]{1,0:T(8,128)(2,1)} %get-tuple-element.49.refs_0_), channel_id=1, source_target_pairs={{0,12},{4,0},{8,4},{12,8},{1,13},{5,1},{9,5},{13,9},{2,14},{6,2},{... | collective-permute-start | bytes 442376 | tf_op jit(solution)/shard_map/ppermute | solution.py:299
  8.3 2.7 %fusion.3.gate_ref = f32[256,384]{1,0:T(8,128)} fusion(bf16[256,2048]{1,0:T(8,128)(2,1)} %get-tuple-element.44, bf16[2048,384]{1,0:T(8,128)(2,1)S(1)} %copy-done), kind=kOutput, calls=%fused_computation.4 | convolution fusion | flops 402653184 | bytes 3014656 | tf_op jit(solution)/shard_map/dot_general | solution.py:332
  11.0 6.8 %project_store.1 = (bf16[1024,256]{1,0:T(8,128)(2,1)}, bf16[1024,256]{1,0:T(8,128)(2,1)}) custom-call(bf16[1024,2048]{1,0:T(8,128)(2,1)} %bitcast.13, f32[1,2048]{1,0:T(1,128)} %bitcast.14, bf16[2048,256]{1,0:T(8,128)(2,1)} %wk_ref.1, bf16[2048,256]{1,0:T(8,128)(2,1)} %wv_ref.1), custom_call_target="tpu_custom_call" | custom-call | flops 2147483648 | bytes 7340032 | tf_op jit(solution)/shard_map/project_store/pallas_call | solution.py:110
  17.8 0.6 copy-done.12
  18.4 0.1 copy-done.13
  18.5 0.1 copy-done.14
  18.5 4.4 %attend.2 = (bf16[144,256]{1,0:T(8,128)(2,1)}, bf16[144,256]{1,0:T(8,128)(2,1)}, bf16[144,256]{1,0:T(8,128)(2,1)}, bf16[144,256]{1,0:T(8,128)(2,1)}) custom-call(bf16[288,256]{1,0:T(8,128)(2,1)} %get-tuple-element.49.refs_0_, bf16[288,256]{1,0:T(8,128)(2,1)} %copy-done.12, bf16[288,256]{1,0:T(8,128)(2,1)} %copy-done.13, bf16[288,256]{1,0:T(8,128)(2,1)} %copy-done.14, ...), custom_call_target="tpu_custom_call" | custom-call | flops 536870912 | bytes 2228224 | tf_op jit(solution)/shard_map/attend/pallas_call | solution.py:178
  22.9 3.0 %fusion.1.mixed_ref = f32[256,384]{1,0:T(8,128)} fusion(bf16[256,2048]{1,0:T(8,128)(2,1)S(1)} %copy-done.1, bf16[2048,384]{1,0:T(8,128)(2,1)} %param.18), kind=kOutput, calls=%fused_computation.2 | convolution fusion | flops 402653184 | bytes 3014656 | tf_op jit(solution)/shard_map/dot_general | solution.py:341
  26.0 1.5 %fusion.2.gated_ref = f32[256,384]{1,0:T(8,128)} fusion(bf16[256,2048]{1,0:T(8,128)(2,1)S(1)} %copy-done.1, bf16[2048,384]{1,0:T(8,128)(2,1)S(1)} %copy-done.2), kind=kOutput, calls=%fused_computation.3 | convolution fusion | flops 402653184 | bytes 3014656 | tf_op jit(solution)/shard_map/dot_general | solution.py:340
  27.4 0.7 %collective-permute-start.4 = (bf16[144,256]{1,0:T(8,128)(2,1)S(1)}, bf16[144,256]{1,0:T(8,128)(2,1)S(1)}, u32[]{:S(2)}, u32[]{:S(2)}) collective-permute-start(bf16[144,256]{1,0:T(8,128)(2,1)S(1)} %copy-done.16), channel_id=1, source_target_pairs={{0,8},{4,12},{8,0},{12,4},{1,9},{5,13},{9,1},{13,5},{2,10},{6,14},... | collective-permute-start | bytes 221192 | tf_op jit(solution)/shard_map/ppermute | solution.py:299
  28.2 1.1 %fusion.refs_4_ = f32[256,256]{1,0:T(8,128)} fusion(bf16[256,2048]{1,0:T(8,128)(2,1)S(1)} %copy-done.1, bf16[2048,256]{1,0:T(8,128)(2,1)S(1)} %copy-done.3), kind=kOutput, calls=%fused_computation.1 | convolution fusion | flops 268435456 | bytes 2359296 | tf_op jit(solution)/shard_map/dot_general | solution.py:342
  29.3 2.5 %mix.1.refs_5_ = bf16[256,384]{1,0:T(8,128)(2,1)} custom-call(f32[256,384]{1,0:T(8,128)} %fusion.1.mixed_ref, f32[256,384]{1,0:T(8,128)} %fusion.2.gated_ref, f32[256,384]{1,0:T(8,128)} %fusion.3.gate_ref, bf16[2,128,128]{2,1,0:T(8,128)(2,1)} %mixw_ref.1), custom_call_target="tpu_custom_call" | custom-call | flops 52297728 | bytes 1376256 | tf_op jit(solution)/shard_map/mix/pallas_call | solution.py:225
  31.8 0.9 %collective-permute-done.4.refs_2_ = bf16[144,256]{1,0:T(8,128)(2,1)S(1)} collective-permute-done((bf16[144,256]{1,0:T(8,128)(2,1)S(1)}, bf16[144,256]{1,0:T(8,128)(2,1)S(1)}, u32[]{:S(2)}, u32[]{:S(2)}) %collective-permute-start.4) | collective-permute-done | bytes 73760 | tf_op jit(solution)/shard_map/ppermute | solution.py:299
  32.6 0.3 collective-permute-done.5.refs_3_
  32.9 0.4 copy-done.8
  33.3 0.6 copy-done.9
  33.9 3.8 %finish.2 = (bf16[64,2048]{1,0:T(8,128)(2,1)}, bf16[64,2048]{1,0:T(8,128)(2,1)}) custom-call(bf16[144,256]{1,0:T(8,128)(2,1)} %get-tuple-element.40.refs_0_, bf16[144,256]{1,0:T(8,128)(2,1)} %copy-done.6, bf16[144,256]{1,0:T(8,128)(2,1)} %copy-done.8, bf16[144,256]{1,0:T(8,128)(2,1)} %copy-done.9, f32[256,256]{1,0:T(8,128)} %fusion.refs_4_, ...), custom_call_target="tpu_custom_call" | custom-call | flops 335544320 | bytes 3145728 | tf_op jit(solution)/shard_map/finish/pallas_call | solution.py:280
  37.7 4.5 %attend.3 = (bf16[144,256]{1,0:T(8,128)(2,1)}, bf16[144,256]{1,0:T(8,128)(2,1)}, bf16[144,256]{1,0:T(8,128)(2,1)}, bf16[144,256]{1,0:T(8,128)(2,1)}) custom-call(bf16[288,256]{1,0:T(8,128)(2,1)} %get-tuple-element.49.refs_0_, bf16[288,256]{1,0:T(8,128)(2,1)} %copy-done.12, bf16[288,256]{1,0:T(8,128)(2,1)} %copy-done.13, bf16[288,256]{1,0:T(8,128)(2,1)} %copy-done.14, ...), custom_call_target="tpu_custom_call" | custom-call | flops 536870912 | bytes 2228224 | tf_op jit(solution)/shard_map/attend/pallas_call | solution.py:178
  42.2 0.6 collective-permute-start.10
  42.8 1.1 %collective-permute-start.8 = (bf16[144,256]{1,0:T(8,128)(2,1)}, bf16[144,256]{1,0:T(8,128)(2,1)S(1)}, u32[]{:S(2)}, u32[]{:S(2)}) collective-permute-start(bf16[144,256]{1,0:T(8,128)(2,1)} %get-tuple-element.54), channel_id=1, source_target_pairs={{0,12},{4,0},{8,4},{12,8},{1,13},{5,1},{9,5},{13,9},{2,14},{6,2},{... | collective-permute-start | bytes 221192 | tf_op jit(solution)/shard_map/ppermute | solution.py:299
  43.9 1.2 %collective-permute-start.9 = (bf16[144,256]{1,0:T(8,128)(2,1)}, bf16[144,256]{1,0:T(8,128)(2,1)S(1)}, u32[]{:S(2)}, u32[]{:S(2)}) collective-permute-start(bf16[144,256]{1,0:T(8,128)(2,1)} %get-tuple-element.55), channel_id=1, source_target_pairs={{0,8},{4,12},{8,0},{12,4},{1,9},{5,13},{9,1},{13,5},{2,10},{6,14},... | collective-permute-start | bytes 221192 | tf_op jit(solution)/shard_map/ppermute | solution.py:299
  45.1 2.9 %collective-permute-start.6 = (bf16[64,2048]{1,0:T(8,128)(2,1)S(1)}, bf16[64,2048]{1,0:T(8,128)(2,1)S(1)}, u32[]{:S(2)}, u32[]{:S(2)}) collective-permute-start(bf16[64,2048]{1,0:T(8,128)(2,1)S(1)} %copy-done.11), channel_id=1, source_target_pairs={{0,2},{1,3},{2,0},{3,1},{4,6},{5,7},{6,4},{7,5},{8,10},{9,11},{10,... | collective-permute-start | bytes 786440 | tf_op jit(solution)/shard_map/ppermute | solution.py:305
  48.0 1.4 %collective-permute-start.7 = (bf16[64,2048]{1,0:T(8,128)(2,1)S(1)}, bf16[64,2048]{1,0:T(8,128)(2,1)S(1)}, u32[]{:S(2)}, u32[]{:S(2)}) collective-permute-start(bf16[64,2048]{1,0:T(8,128)(2,1)S(1)} %copy-done.10), channel_id=1, source_target_pairs={{0,3},{1,2},{2,1},{3,0},{4,7},{5,6},{6,5},{7,4},{8,11},{9,10},{10,... | collective-permute-start | bytes 786440 | tf_op jit(solution)/shard_map/ppermute | solution.py:305
  49.4 0.6 copy-done.4
  50.0 3.8 %finish.3 = (bf16[64,2048]{1,0:T(8,128)(2,1)}, bf16[64,2048]{1,0:T(8,128)(2,1)}) custom-call(bf16[144,256]{1,0:T(8,128)(2,1)} %get-tuple-element.53.refs_0_, bf16[144,256]{1,0:T(8,128)(2,1)} %copy-done.5, bf16[144,256]{1,0:T(8,128)(2,1)} %copy-done.7, bf16[144,256]{1,0:T(8,128)(2,1)} %copy-done.4, f32[256,256]{1,0:T(8,128)} %fusion.refs_4_, ...), custom_call_target="tpu_custom_call" | custom-call | flops 335544320 | bytes 3145728 | tf_op jit(solution)/shard_map/finish/pallas_call | solution.py:280
  53.9 1.1 %collective-permute-start.11 = (bf16[64,2048]{1,0:T(8,128)(2,1)}, bf16[64,2048]{1,0:T(8,128)(2,1)S(1)}, u32[]{:S(2)}, u32[]{:S(2)}) collective-permute-start(bf16[64,2048]{1,0:T(8,128)(2,1)} %get-tuple-element.58), channel_id=1, source_target_pairs={{0,1},{1,0},{2,3},{3,2},{4,5},{5,4},{6,7},{7,6},{8,9},{9,8},{10,11... | collective-permute-start | bytes 786440 | tf_op jit(solution)/shard_map/ppermute | solution.py:305
  55.0 10.6 %collective-permute-done.6 = bf16[64,2048]{1,0:T(8,128)(2,1)S(1)} collective-permute-done((bf16[64,2048]{1,0:T(8,128)(2,1)S(1)}, bf16[64,2048]{1,0:T(8,128)(2,1)S(1)}, u32[]{:S(2)}, u32[]{:S(2)}) %collective-permute-start.6) | collective-permute-done | bytes 262176 | tf_op jit(solution)/shard_map/ppermute | solution.py:305
  65.6 3.7 %collective-permute-done.11 = bf16[64,2048]{1,0:T(8,128)(2,1)S(1)} collective-permute-done((bf16[64,2048]{1,0:T(8,128)(2,1)}, bf16[64,2048]{1,0:T(8,128)(2,1)S(1)}, u32[]{:S(2)}, u32[]{:S(2)}) %collective-permute-start.11) | collective-permute-done | bytes 262176 | tf_op jit(solution)/shard_map/ppermute | solution.py:305
  69.3 1.8 %add_convert_fusion = bf16[64,2048]{1,0:T(8,128)(2,1)} fusion(bf16[64,2048]{1,0:T(8,128)(2,1)S(1)} %collective-permute-done.11, bf16[64,2048]{1,0:T(8,128)(2,1)} %get-tuple-element.57, bf16[64,2048]{1,0:T(8,128)(2,1)S(1)} %collective-permute-done.7, bf16[64,2048]{1,0:T(8,128)(2,1)S(1)} %collective-permute-done.6), kind=kLoop, calls=%fused_computation | loop fusion | flops 1048576 | bytes 1310720 | tf_op jit(solution)/shard_map/convert_element_type | solution.py:349
  (40 shorter events, 0.1 us)
Async XLA Ops:
  0.0 8.3 %copy-start = (bf16[2048,384]{1,0:T(8,128)(2,1)S(1)}, bf16[2048,384]{1,0:T(8,128)(2,1)}, u32[]{:S(2)}) copy-start(bf16[2048,384]{1,0:T(8,128)(2,1)} %param.21) | copy-start | bytes 4718596
  3.8 13.9 %collective-permute-start = (bf16[288,256]{1,0:T(8,128)(2,1)}, bf16[288,256]{1,0:T(8,128)(2,1)S(1)}, u32[]{:S(2)}, u32[]{:S(2)}) collective-permute-start(bf16[288,256]{1,0:T(8,128)(2,1)} %get-tuple-element.49.refs_0_), channel_id=1, source_target_pairs={{0,4},{4,8},{8,12},{12,0},{1,5},{5,9},{9,13},{13,1},{2,6},{6,10},{... | collective-permute-start | bytes 442376 | tf_op jit(solution)/shard_map/ppermute | solution.py:299
  4.3 13.5 %collective-permute-start.1 = (bf16[288,256]{1,0:T(8,128)(2,1)}, bf16[288,256]{1,0:T(8,128)(2,1)S(1)}, u32[]{:S(2)}, u32[]{:S(2)}) collective-permute-start(bf16[288,256]{1,0:T(8,128)(2,1)} %get-tuple-element.49.refs_0_), channel_id=1, source_target_pairs={{0,8},{4,12},{8,0},{12,4},{1,9},{5,13},{9,1},{13,5},{2,10},{6,14},... | collective-permute-start | bytes 442376 | tf_op jit(solution)/shard_map/ppermute | solution.py:299
  6.8 10.9 %collective-permute-start.2 = (bf16[288,256]{1,0:T(8,128)(2,1)}, bf16[288,256]{1,0:T(8,128)(2,1)S(1)}, u32[]{:S(2)}, u32[]{:S(2)}) collective-permute-start(bf16[288,256]{1,0:T(8,128)(2,1)} %get-tuple-element.49.refs_0_), channel_id=1, source_target_pairs={{0,12},{4,0},{8,4},{12,8},{1,13},{5,1},{9,5},{13,9},{2,14},{6,2},{... | collective-permute-start | bytes 442376 | tf_op jit(solution)/shard_map/ppermute | solution.py:299
  17.7 5.2 %copy-start.1 = (bf16[256,2048]{1,0:T(8,128)(2,1)S(1)}, bf16[256,2048]{1,0:T(8,128)(2,1)}, u32[]{:S(2)}) copy-start(bf16[256,2048]{1,0:T(8,128)(2,1)} %get-tuple-element.44) | copy-start | bytes 3145732
  17.8 0.7 copy-start.12
  17.8 0.7 copy-start.13
  17.8 0.7 %copy-start.14 = (bf16[288,256]{1,0:T(8,128)(2,1)}, bf16[288,256]{1,0:T(8,128)(2,1)S(1)}, u32[]{:S(2)}) copy-start(bf16[288,256]{1,0:T(8,128)(2,1)S(1)} %collective-permute-done.2.refs_3_) | copy-start | bytes 442372
  22.9 3.0 %copy-start.2 = (bf16[2048,384]{1,0:T(8,128)(2,1)S(1)}, bf16[2048,384]{1,0:T(8,128)(2,1)}, u32[]{:S(2)}) copy-start(bf16[2048,384]{1,0:T(8,128)(2,1)} %param.17) | copy-start | bytes 4718596
  25.9 1.5 %copy-start.17 = (bf16[144,256]{1,0:T(8,128)(2,1)S(1)}, bf16[144,256]{1,0:T(8,128)(2,1)}, u32[]{:S(2)}) copy-start(bf16[144,256]{1,0:T(8,128)(2,1)} %get-tuple-element.41) | copy-start | bytes 221188
  25.9 1.5 %copy-start.16 = (bf16[144,256]{1,0:T(8,128)(2,1)S(1)}, bf16[144,256]{1,0:T(8,128)(2,1)}, u32[]{:S(2)}) copy-start(bf16[144,256]{1,0:T(8,128)(2,1)} %get-tuple-element.42) | copy-start | bytes 221188
  25.9 2.2 %copy-start.15 = (bf16[144,256]{1,0:T(8,128)(2,1)S(1)}, bf16[144,256]{1,0:T(8,128)(2,1)}, u32[]{:S(2)}) copy-start(bf16[144,256]{1,0:T(8,128)(2,1)} %get-tuple-element.43) | copy-start | bytes 221188
  25.9 2.2 %copy-start.3 = (bf16[2048,256]{1,0:T(8,128)(2,1)S(1)}, bf16[2048,256]{1,0:T(8,128)(2,1)}, u32[]{:S(2)}) copy-start(bf16[2048,256]{1,0:T(8,128)(2,1)} %param.22) | copy-start | bytes 3145732
  27.4 4.3 %collective-permute-start.3 = (bf16[144,256]{1,0:T(8,128)(2,1)S(1)}, bf16[144,256]{1,0:T(8,128)(2,1)S(1)}, u32[]{:S(2)}, u32[]{:S(2)}) collective-permute-start(bf16[144,256]{1,0:T(8,128)(2,1)S(1)} %copy-done.17), channel_id=1, source_target_pairs={{0,12},{4,0},{8,4},{12,8},{1,13},{5,1},{9,5},{13,9},{2,14},{6,2},{... | collective-permute-start | bytes 221192 | tf_op jit(solution)/shard_map/ppermute | solution.py:299
  27.4 5.2 %collective-permute-start.4 = (bf16[144,256]{1,0:T(8,128)(2,1)S(1)}, bf16[144,256]{1,0:T(8,128)(2,1)S(1)}, u32[]{:S(2)}, u32[]{:S(2)}) collective-permute-start(bf16[144,256]{1,0:T(8,128)(2,1)S(1)} %copy-done.16), channel_id=1, source_target_pairs={{0,8},{4,12},{8,0},{12,4},{1,9},{5,13},{9,1},{13,5},{2,10},{6,14},... | collective-permute-start | bytes 221192 | tf_op jit(solution)/shard_map/ppermute | solution.py:299
  28.2 4.7 %collective-permute-start.5 = (bf16[144,256]{1,0:T(8,128)(2,1)S(1)}, bf16[144,256]{1,0:T(8,128)(2,1)S(1)}, u32[]{:S(2)}, u32[]{:S(2)}) collective-permute-start(bf16[144,256]{1,0:T(8,128)(2,1)S(1)} %copy-done.15), channel_id=1, source_target_pairs={{0,4},{4,8},{8,12},{12,0},{1,5},{5,9},{9,13},{13,1},{2,6},{6,10},{... | collective-permute-start | bytes 221192 | tf_op jit(solution)/shard_map/ppermute | solution.py:299
  31.8 1.1 %copy-start.6 = (bf16[144,256]{1,0:T(8,128)(2,1)}, bf16[144,256]{1,0:T(8,128)(2,1)S(1)}, u32[]{:S(2)}) copy-start(bf16[144,256]{1,0:T(8,128)(2,1)S(1)} %collective-permute-done.3.refs_1_) | copy-start | bytes 221188
  32.6 0.6 copy-start.8
  33.3 0.6 copy-start.9
  37.7 7.4 %copy-start.11 = (bf16[64,2048]{1,0:T(8,128)(2,1)S(1)}, bf16[64,2048]{1,0:T(8,128)(2,1)}, u32[]{:S(2)}) copy-start(bf16[64,2048]{1,0:T(8,128)(2,1)} %get-tuple-element.47) | copy-start | bytes 786436
  37.7 10.3 %copy-start.10 = (bf16[64,2048]{1,0:T(8,128)(2,1)S(1)}, bf16[64,2048]{1,0:T(8,128)(2,1)}, u32[]{:S(2)}) copy-start(bf16[64,2048]{1,0:T(8,128)(2,1)} %get-tuple-element.48) | copy-start | bytes 786436
  42.2 7.2 %collective-permute-start.10 = (bf16[144,256]{1,0:T(8,128)(2,1)}, bf16[144,256]{1,0:T(8,128)(2,1)S(1)}, u32[]{:S(2)}, u32[]{:S(2)}) collective-permute-start(bf16[144,256]{1,0:T(8,128)(2,1)} %get-tuple-element.56), channel_id=1, source_target_pairs={{0,4},{4,8},{8,12},{12,0},{1,5},{5,9},{9,13},{13,1},{2,6},{6,10},{... | collective-permute-start | bytes 221192 | tf_op jit(solution)/shard_map/ppermute | solution.py:299
  42.8 6.5 %collective-permute-start.8 = (bf16[144,256]{1,0:T(8,128)(2,1)}, bf16[144,256]{1,0:T(8,128)(2,1)S(1)}, u32[]{:S(2)}, u32[]{:S(2)}) collective-permute-start(bf16[144,256]{1,0:T(8,128)(2,1)} %get-tuple-element.54), channel_id=1, source_target_pairs={{0,12},{4,0},{8,4},{12,8},{1,13},{5,1},{9,5},{13,9},{2,14},{6,2},{... | collective-permute-start | bytes 221192 | tf_op jit(solution)/shard_map/ppermute | solution.py:299
  43.9 5.4 %collective-permute-start.9 = (bf16[144,256]{1,0:T(8,128)(2,1)}, bf16[144,256]{1,0:T(8,128)(2,1)S(1)}, u32[]{:S(2)}, u32[]{:S(2)}) collective-permute-start(bf16[144,256]{1,0:T(8,128)(2,1)} %get-tuple-element.55), channel_id=1, source_target_pairs={{0,8},{4,12},{8,0},{12,4},{1,9},{5,13},{9,1},{13,5},{2,10},{6,14},... | collective-permute-start | bytes 221192 | tf_op jit(solution)/shard_map/ppermute | solution.py:299
  45.1 20.4 %collective-permute-start.6 = (bf16[64,2048]{1,0:T(8,128)(2,1)S(1)}, bf16[64,2048]{1,0:T(8,128)(2,1)S(1)}, u32[]{:S(2)}, u32[]{:S(2)}) collective-permute-start(bf16[64,2048]{1,0:T(8,128)(2,1)S(1)} %copy-done.11), channel_id=1, source_target_pairs={{0,2},{1,3},{2,0},{3,1},{4,6},{5,7},{6,4},{7,5},{8,10},{9,11},{10,... | collective-permute-start | bytes 786440 | tf_op jit(solution)/shard_map/ppermute | solution.py:305
  48.0 17.6 %collective-permute-start.7 = (bf16[64,2048]{1,0:T(8,128)(2,1)S(1)}, bf16[64,2048]{1,0:T(8,128)(2,1)S(1)}, u32[]{:S(2)}, u32[]{:S(2)}) collective-permute-start(bf16[64,2048]{1,0:T(8,128)(2,1)S(1)} %copy-done.10), channel_id=1, source_target_pairs={{0,3},{1,2},{2,1},{3,0},{4,7},{5,6},{6,5},{7,4},{8,11},{9,10},{10,... | collective-permute-start | bytes 786440 | tf_op jit(solution)/shard_map/ppermute | solution.py:305
  49.4 0.6 copy-start.4
  49.4 0.6 copy-start.5
  49.4 0.7 copy-start.7
  53.9 15.4 %collective-permute-start.11 = (bf16[64,2048]{1,0:T(8,128)(2,1)}, bf16[64,2048]{1,0:T(8,128)(2,1)S(1)}, u32[]{:S(2)}, u32[]{:S(2)}) collective-permute-start(bf16[64,2048]{1,0:T(8,128)(2,1)} %get-tuple-element.58), channel_id=1, source_target_pairs={{0,1},{1,0},{2,3},{3,2},{4,5},{5,4},{6,7},{7,6},{8,9},{9,8},{10,11... | collective-permute-start | bytes 786440 | tf_op jit(solution)/shard_map/ppermute | solution.py:305
